TPU v7x, 32 devices: a whole 2x2x4 slice. The times are simulated.
32 devices in a mesh: grp: 2 (over y), fs: 4 (over z), tp: 4 (over x, core).
Axes of the slice: x: 2, y: 2, z: 4, core: 2. Of those that a mesh axis runs over, the one named last changes fastest.
Arguments:
- tokens: bfloat16 [4096, 2048], P(('grp', 'fs', 'tp')), parts along dimension 0, may hold values from -6 to 6
- route_ids: int32 [4096, 8], P(('grp', 'fs', 'tp')), parts along dimension 0, may hold values from 0 to 15, all different within a row; in each aligned block of 128 rows (0 to 127, 128 to 255, ...) at most 96 rows name the same one
- route_scores: float32 [4096, 8], P(('grp', 'fs', 'tp')), parts along dimension 0, may hold values from 0.05 to 1
- norm_gain: float32 [2048], P('fs'), may hold values from 0.1 to 1.9
- expert_gate: float32 [16, 2048, 256], P(None, 'fs', 'tp'), may hold values from -0.125 to 0.125
- expert_up: float32 [16, 2048, 256], P(None, 'fs', 'tp'), may hold values from -0.125 to 0.125
- expert_down: float32 [16, 256, 2048], P(None, 'fs', 'tp'), may hold values from -0.375 to 0.375
- shared_gate: float32 [2048, 256], P('fs', 'tp'), may hold values from -0.125 to 0.125
- shared_up: float32 [2048, 256], P('fs', 'tp'), may hold values from -0.125 to 0.125
- shared_down: float32 [256, 2048], P('fs', 'tp'), may hold values from -0.375 to 0.375
Outputs:
- mixed: bfloat16 [4096, 2048], P(('grp', 'fs', 'tp')), parts along dimension 0
- sampler_gate: bfloat16 [32, 2048, 256], P(('grp', 'fs', 'tp')), parts along dimension 0
- sampler_up: bfloat16 [32, 2048, 256], P(('grp', 'fs', 'tp')), parts along dimension 0
- sampler_down: bfloat16 [32, 256, 2048], P(('grp', 'fs', 'tp')), parts along dimension 0
- sampler_shared_gate: bfloat16 [4096, 256], P(('grp', 'fs')), parts along dimension 0
- sampler_shared_up: bfloat16 [4096, 256], P(('grp', 'fs')), parts along dimension 0
- sampler_shared_down: bfloat16 [512, 2048], P(('grp', 'fs')), parts along dimension 0
There are 2 independent parts, one for each index of `grp`. A program takes and returns all parts, laid end to end along the dimension named above; an argument that names none is the same for every part. Nothing has to cross between parts.
Inputs may be any that keep to these rules, and one draw needn't show every extreme that they name: `route_ids`: each row names 8 different experts. Among the 128 rows of one device no expert is named more than 96 times, a bound that some block reaches.
All inputs are finite; a program needn't handle non-finite values.
Results may differ from a plain program's by a relative error of at most 0.0084.
Values may be sent and summed in bfloat16 or wider, within the bound.
No kernel may reach another device: no remote copies, remote signals or barrier semaphores. Data moves between devices by JAX's collectives and lax.ppermute only.
A program may use at most 128 MiB of HBM per device.

v0:
```python
import jax
import jax.numpy as jnp
from jax import lax
from jax.sharding import PartitionSpec as P

EPSILON = 1e-06
route_scale = 2.5


def expert_rows(row_block, w_gate, w_up, w_down):
    gate_rows = jnp.dot(row_block, w_gate, preferred_element_type=jnp.float32)
    up_rows = jnp.dot(row_block, w_up, preferred_element_type=jnp.float32)
    hidden = (jax.nn.silu(gate_rows) * up_rows).astype(jnp.bfloat16)
    return jnp.dot(hidden, w_down, preferred_element_type=jnp.float32).astype(jnp.bfloat16)


def relayout(arrived, fs_count, tp_count):
    tile_rows = arrived.shape[2]
    tile_cols = arrived.shape[3]
    grid = arrived.reshape(fs_count, tp_count, tile_rows, tile_cols)
    grid = jnp.transpose(grid, (0, 2, 1, 3))
    return grid.reshape(1, fs_count * tile_rows, tp_count * tile_cols)


def on_device(
    tokens,
    route_ids,
    route_scores,
    norm_gain,
    expert_gate,
    expert_up,
    expert_down,
    shared_gate,
    shared_up,
    shared_down,
):
    fs_count = lax.axis_size("fs")
    tp_count = lax.axis_size("tp")
    experts = fs_count * tp_count
    gain_col = norm_gain[:, None]
    piece_gate = (gain_col[None] * expert_gate).astype(jnp.bfloat16)
    piece_up = (gain_col[None] * expert_up).astype(jnp.bfloat16)
    piece_down = expert_down.astype(jnp.bfloat16)
    moved = (
        lax.all_to_all(piece_gate[:, None], ("fs", "tp"), split_axis=0, concat_axis=1, tiled=True),
        lax.all_to_all(piece_up[:, None], ("fs", "tp"), split_axis=0, concat_axis=1, tiled=True),
        lax.all_to_all(piece_down[:, None], ("fs", "tp"), split_axis=0, concat_axis=1, tiled=True),
    )
    served_gate = relayout(moved[0], fs_count, tp_count)
    served_up = relayout(moved[1], fs_count, tp_count)
    served_down = relayout(moved[2], fs_count, tp_count)
    tile_gate = (gain_col * shared_gate).astype(jnp.bfloat16)
    tile_up = (gain_col * shared_up).astype(jnp.bfloat16)
    tile_down = shared_down.astype(jnp.bfloat16)
    held_gate, held_up, held_down = (
        lax.all_gather(tile_gate, "tp", axis=1, tiled=True),
        lax.all_gather(tile_up, "tp", axis=1, tiled=True),
        lax.all_gather(tile_down, "tp", axis=1, tiled=True),
    )
    rows_dev = tokens.shape[0]
    width = tokens.shape[1]
    picks = route_ids.shape[1]
    capacity = 3 * rows_dev * picks // (2 * experts)
    widened = tokens.astype(jnp.float32)
    normed = (
        widened * lax.rsqrt(jnp.mean(widened * widened, axis=1, keepdims=True) + EPSILON)
    ).astype(jnp.bfloat16)
    weights = route_scale * route_scores / jnp.sum(route_scores, axis=1, keepdims=True)
    flat_ids = route_ids.reshape(-1)
    onehot = (flat_ids[:, None] == jnp.arange(experts, dtype=jnp.int32)[None, :]).astype(jnp.int32)
    earlier = jnp.cumsum(onehot, axis=0) - onehot
    ranks = jnp.sum(earlier * onehot, axis=1)
    target = flat_ids * capacity + ranks
    outbox = (
        jnp.zeros((experts * capacity, width), jnp.bfloat16)
        .at[target]
        .set(jnp.repeat(normed, picks, axis=0))
    )
    arrived = lax.all_to_all(
        outbox.reshape(experts, capacity, width),
        ("fs", "tp"),
        split_axis=0,
        concat_axis=0,
        tiled=True,
    )
    finished = expert_rows(
        arrived.reshape(-1, width), served_gate[0], served_up[0], served_down[0]
    ).reshape(arrived.shape)
    returned = lax.all_to_all(finished, ("fs", "tp"), split_axis=0, concat_axis=0, tiled=True)
    results = returned.reshape(experts * capacity, width)[target]
    routed = jnp.sum(
        results.reshape(rows_dev, picks, width).astype(jnp.float32) * weights[:, :, None], axis=1
    )
    columns = normed
    gate_part = jnp.dot(
        columns,
        lax.all_gather(held_gate, "fs", axis=0, tiled=True),
        preferred_element_type=jnp.float32,
    )
    up_part = jnp.dot(
        columns,
        lax.all_gather(held_up, "fs", axis=0, tiled=True),
        preferred_element_type=jnp.float32,
    )
    shared_hidden = (jax.nn.silu(gate_part) * up_part).astype(jnp.bfloat16)
    columns = shared_hidden
    shared_term = jnp.dot(
        columns,
        lax.all_gather(held_down, "fs", axis=0, tiled=True),
        preferred_element_type=jnp.float32,
    )
    mixed = (routed + shared_term).astype(jnp.bfloat16)
    return (mixed, served_gate, served_up, served_down, held_gate, held_up, held_down)


def solution(mesh):
    return jax.shard_map(
        on_device,
        mesh=mesh,
        in_specs=(
            P(("grp", "fs", "tp"), None),
            P(("grp", "fs", "tp"), None),
            P(("grp", "fs", "tp"), None),
            P("fs"),
            P(None, "fs", "tp"),
            P(None, "fs", "tp"),
            P(None, "fs", "tp"),
            P("fs", "tp"),
            P("fs", "tp"),
            P("fs", "tp"),
        ),
        out_specs=(
            P(("grp", "fs", "tp"), None),
            P(("grp", "fs", "tp"), None, None),
            P(("grp", "fs", "tp"), None, None),
            P(("grp", "fs", "tp"), None, None),
            P(("grp", "fs"), None),
            P(("grp", "fs"), None),
            P(("grp", "fs"), None),
        ),
        check_vma=False,
    )
```

profile of v0, /device:TPU:11, one launch (start us, length us, event | category | flops | bytes accessed | tf_op | source)
XLA Modules:
  0.0 485.5 jit_solution(11063605218181208656)
XLA Ops:
  7.2 3.8 fusion.10
  11.0 31.1 %all_to_all.37 = bf16[16,1,512,64]{2,3,1,0:T(8,128)(2,1)S(1)} all-to-all(bf16[16,1,512,64]{2,3,1,0:T(8,128)(2,1)S(1)} %get-tuple-element.36), channel_id=1, replica_groups=mesh['grp'=2,'fs'=4,'tp'=4] {'fs','tp'}, dimensions={0} | all-to-all | bytes 2097152 | tf_op jit(solution)/shard_map/all_to_all | solution.py:45
  42.1 5.0 %all-to-all-start.2 = ((bf16[16,1,512,64]{2,3,1,0:T(8,128)(2,1)}), bf16[16,1,512,64]{2,3,1,0:T(8,128)(2,1)S(1)}, u32[]{:S(2)}, u32[]{:S(2)}) async-start(bf16[16,1,512,64]{2,3,1,0:T(8,128)(2,1)} %get-tuple-element.37), calls=%async_computation.2 | async-start | bytes 2097152 | tf_op jit(solution)/shard_map/all_to_all | solution.py:46
  47.1 2.7 convert_bitcast_fusion
  49.9 22.1 %all-to-all-done.2 = bf16[16,1,512,64]{2,3,1,0:T(8,128)(2,1)S(1)} async-done(((bf16[16,1,512,64]{2,3,1,0:T(8,128)(2,1)}), bf16[16,1,512,64]{2,3,1,0:T(8,128)(2,1)S(1)}, u32[]{:S(2)}, u32[]{:S(2)}) %all-to-all-start.2) | async-done | bytes 1048608 | tf_op jit(solution)/shard_map/all_to_all | solution.py:46
  72.0 4.8 all-to-all-start.3
  77.1 4.5 reduce-window.6
  82.7 10.2 %scatter_custom_fusion = bf16[1536,2048]{1,0:T(8,128)(2,1)} fusion(s32[1024]{0:T(1024)S(1)} %bitcast.93, bf16[]{:T(256)} %constant.9.clone.1, bf16[128,2048]{1,0:T(8,128)(2,1)S(1)} %fusion.9), kind=kCustom, calls=%fused_computation.5 | custom fusion | bytes 6815746 | tf_op jit(solution)/shard_map/scatter | solution.py:77
  92.9 8.9 %all-to-all-done.3 = bf16[16,1,64,512]{3,2,1,0:T(8,128)(2,1)} async-done(((bf16[16,1,64,512]{3,2,1,0:T(8,128)(2,1)}), bf16[16,1,64,512]{3,2,1,0:T(8,128)(2,1)}, u32[]{:S(2)}, u32[]{:S(2)}) %all-to-all-start.3) | async-done | bytes 1048608 | tf_op jit(solution)/shard_map/all_to_all | solution.py:47
  101.8 4.8 all-to-all-start
  110.8 2.0 copy.77
  114.0 130.0 %all-to-all-done = bf16[16,96,2048]{2,1,0:T(8,128)(2,1)} async-done(((bf16[16,96,2048]{2,1,0:T(8,128)(2,1)}), bf16[16,96,2048]{2,1,0:T(8,128)(2,1)}, u32[]{:S(2)}, u32[]{:S(2)}) %all-to-all-start) | async-done | bytes 6291488 | tf_op jit(solution)/shard_map/all_to_all | solution.py:79
  244.0 6.1 %fusion.25 = f32[1536,256]{1,0:T(8,128)} fusion(bf16[1536,2048]{1,0:T(8,128)(2,1)} %bitcast.6, bf16[2048,256]{0,1:T(8,128)(2,1)} %bitcast.87), kind=kOutput, calls=%fused_computation.51 | convolution fusion | flops 1610612736 | bytes 8912896 | tf_op jit(solution)/shard_map/dot_general | solution.py:11
  250.1 12.9 %convolution_convert_fusion = bf16[1536,2048]{1,0:T(8,128)(2,1)} fusion(bf16[256,2048]{1,0:T(8,128)(2,1)} %bitcast.89, bf16[1536,2048]{1,0:T(8,128)(2,1)} %bitcast.6, bf16[2048,256]{0,1:T(8,128)(2,1)} %bitcast.88, f32[1536,256]{1,0:T(8,128)} %fusion.25), kind=kOutput, calls=%fused_computation.4 | convolution fusion | flops 3226730496 | bytes 16252928 | tf_op jit(solution)/shard_map/dot_general | solution.py:14
  263.0 4.9 %all-to-all-start.4 = ((bf16[16,96,2048]{2,1,0:T(8,128)(2,1)}), bf16[16,96,2048]{2,1,0:T(8,128)(2,1)}, u32[]{:S(2)}, u32[]{:S(2)}) async-start(bf16[16,96,2048]{2,1,0:T(8,128)(2,1)} %bitcast.84), calls=%async_computation.4 | async-start | bytes 12582912 | tf_op jit(solution)/shard_map/all_to_all | solution.py:89
  268.0 29.8 %all_gather.18 = bf16[512,256]{0,1:T(8,128)(2,1)} all-gather(bf16[512,64]{0,1:T(8,128)(2,1)S(1)} %get-tuple-element.34), channel_id=1, replica_groups=mesh['grp'=2,'fs'=4,'tp'=4] {'tp'}, dimensions={1}, use_global_device_ids=true | all-gather | bytes 327680 | tf_op jit(solution)/shard_map/all_gather | solution.py:56
  298.0 10.4 %all_gather.20 = bf16[512,256]{0,1:T(8,128)(2,1)} all-gather(bf16[512,64]{0,1:T(8,128)(2,1)S(1)} %get-tuple-element.35), channel_id=1, replica_groups=mesh['grp'=2,'fs'=4,'tp'=4] {'tp'}, dimensions={1}, use_global_device_ids=true | all-gather | bytes 327680 | tf_op jit(solution)/shard_map/all_gather | solution.py:57
  309.3 8.1 %all_gather.22 = bf16[64,2048]{1,0:T(8,128)(2,1)} all-gather(bf16[64,512]{1,0:T(8,128)(2,1)S(1)} %convert_element_type.63), channel_id=1, replica_groups=mesh['grp'=2,'fs'=4,'tp'=4] {'tp'}, dimensions={1}, use_global_device_ids=true | all-gather | bytes 327680 | tf_op jit(solution)/shard_map/all_gather | solution.py:58
  321.1 52.7 %all-gather.4.cloned.1.call-done = bf16[2048,256]{0,1:T(8,128)(2,1)} async-done(((bf16[512,256]{0,1:T(8,128)(2,1)}), bf16[2048,256]{0,1:T(8,128)(2,1)}) %all-gather.4.cloned.1.call-update) | async-done | bytes 1048592 | tf_op jit(solution)/shard_map/all_gather | solution.py:97
  377.3 2.3 copy.62
  383.2 72.7 %all-to-all-done.4 = bf16[16,96,2048]{2,1,0:T(8,128)(2,1)} async-done(((bf16[16,96,2048]{2,1,0:T(8,128)(2,1)}), bf16[16,96,2048]{2,1,0:T(8,128)(2,1)}, u32[]{:S(2)}, u32[]{:S(2)}) %all-to-all-start.4) | async-done | bytes 6291488 | tf_op jit(solution)/shard_map/all_to_all | solution.py:89
  455.9 12.4 %gather_fusion = bf16[1024,2048]{1,0:T(8,128)(2,1)} fusion(bf16[1536,2048]{1,0:T(8,128)(2,1)} %bitcast.18, s32[1024]{0:T(1024)S(1)} %broadcast_clamp_fusion), kind=kCustom, calls=%fused_computation | custom fusion | bytes 8392704 | tf_op jit(solution)/shard_map/gather | solution.py:90
  468.4 6.5 %fusion = f32[128,2048]{1,0:T(8,128)S(1)} fusion(bf16[1024,2048]{1,0:T(8,128)(2,1)} %gather_fusion, f32[128,8]{1,0:T(8,128)S(1)} %copy.61), kind=kLoop, calls=%fused_computation.3 | loop fusion | flops 6029312 | bytes 5246976 | tf_op jit(solution)/shard_map/reduce_sum | solution.py:91
  475.0 3.3 fusion.5
  (63 shorter events, 19.4 us)
Async XLA Ops:
  42.1 34.7 %copy-start.6 = (s32[128,8]{0,1:T(8,128)S(1)}, s32[128,8]{0,1:T(8,128)}, u32[]{:S(2)}) copy-start(s32[128,8]{0,1:T(8,128)} %param.11) | copy-start | bytes 12292
  42.1 40.2 %copy-start.3 = (bf16[128,2048]{1,0:T(8,128)(2,1)S(1)}, bf16[128,2048]{1,0:T(8,128)(2,1)}, u32[]{:S(2)}) copy-start(bf16[128,2048]{1,0:T(8,128)(2,1)} %param.10) | copy-start | bytes 1572868
  42.1 29.9 %all-to-all-start.2 = ((bf16[16,1,512,64]{2,3,1,0:T(8,128)(2,1)}), bf16[16,1,512,64]{2,3,1,0:T(8,128)(2,1)S(1)}, u32[]{:S(2)}, u32[]{:S(2)}) async-start(bf16[16,1,512,64]{2,3,1,0:T(8,128)(2,1)} %get-tuple-element.37), calls=%async_computation.2 | async-start | bytes 2097152 | tf_op jit(solution)/shard_map/all_to_all | solution.py:46
  72.0 29.8 %all-to-all-start.3 = ((bf16[16,1,64,512]{3,2,1,0:T(8,128)(2,1)}), bf16[16,1,64,512]{3,2,1,0:T(8,128)(2,1)}, u32[]{:S(2)}, u32[]{:S(2)}) async-start(bf16[16,1,64,512]{3,2,1,0:T(8,128)(2,1)} %convert_bitcast_fusion), calls=%async_computation.3 | async-start | bytes 2097152 | tf_op jit(solution)/shard_map/all_to_all | solution.py:47
  82.7 19.1 %copy-start = (bf16[128,2048]{1,0:T(8,128)(2,1)}, bf16[128,2048]{1,0:T(8,128)(2,1)S(1)}, u32[]{:S(2)}) copy-start(bf16[128,2048]{1,0:T(8,128)(2,1)S(1)} %fusion.9) | copy-start | bytes 1572868
  101.8 142.2 %all-to-all-start = ((bf16[16,96,2048]{2,1,0:T(8,128)(2,1)}), bf16[16,96,2048]{2,1,0:T(8,128)(2,1)}, u32[]{:S(2)}, u32[]{:S(2)}) async-start(bf16[16,96,2048]{2,1,0:T(8,128)(2,1)} %bitcast.77), calls=%async_computation | async-start | bytes 12582912 | tf_op jit(solution)/shard_map/all_to_all | solution.py:79
  263.0 5.0 %copy-start.4 = (f32[512,64]{0,1:T(8,128)S(1)}, f32[512,64]{0,1:T(8,128)}, u32[]{:S(2)}) copy-start(f32[512,64]{0,1:T(8,128)} %param.17) | copy-start | bytes 393220
  263.0 5.0 %copy-start.5 = (f32[512,64]{0,1:T(8,128)S(1)}, f32[512,64]{0,1:T(8,128)}, u32[]{:S(2)}) copy-start(f32[512,64]{0,1:T(8,128)} %param.18) | copy-start | bytes 393220
  263.0 5.0 %copy-start.8 = (f32[512]{0:T(512)S(1)}, f32[512]{0:T(512)}, u32[]{:S(2)}) copy-start(f32[512]{0:T(512)} %param.13) | copy-start | bytes 6148
  263.0 58.0 %copy-start.7 = (f32[128,8]{0,1:T(8,128)S(1)}, f32[128,8]{0,1:T(8,128)}, u32[]{:S(2)}) copy-start(f32[128,8]{0,1:T(8,128)} %param.12) | copy-start | bytes 12292
  263.0 192.9 %all-to-all-start.4 = ((bf16[16,96,2048]{2,1,0:T(8,128)(2,1)}), bf16[16,96,2048]{2,1,0:T(8,128)(2,1)}, u32[]{:S(2)}, u32[]{:S(2)}) async-start(bf16[16,96,2048]{2,1,0:T(8,128)(2,1)} %bitcast.84), calls=%async_computation.4 | async-start | bytes 12582912 | tf_op jit(solution)/shard_map/all_to_all | solution.py:89
  267.9 105.9 %all-gather.4.cloned.1.call-start = ((), (), s32[]{:S(2)}) async-start(), calls=%async_computation.5 | async-start | bytes 1310720 | tf_op jit(solution)/shard_map/all_gather | solution.py:97
  297.9 177.0 %all-gather.6.cloned.1.call-start = ((), (), s32[]{:S(2)}) async-start(), calls=%async_computation.6 | async-start | bytes 1310720 | tf_op jit(solution)/shard_map/all_gather | solution.py:102
  308.3 166.6 %all-gather.8.cloned.1.call-start = ((), (), s32[]{:S(2)}) async-start(), calls=%async_computation.7 | async-start | bytes 1310720 | tf_op jit(solution)/shard_map/all_gather | solution.py:109
  468.4 6.6 %copy-start.1 = (bf16[128,2048]{1,0:T(8,128)(2,1)S(1)}, bf16[128,2048]{1,0:T(8,128)(2,1)}, u32[]{:S(2)}) copy-start(bf16[128,2048]{1,0:T(8,128)(2,1)} %copy-done) | copy-start | bytes 1572868
  468.4 9.9 %copy-start.2 = (bf16[64,2048]{1,0:T(8,128)(2,1)S(1)}, bf16[64,2048]{1,0:T(8,128)(2,1)}, u32[]{:S(2)}) copy-start(bf16[64,2048]{1,0:T(8,128)(2,1)} %all_gather.22) | copy-start | bytes 786436
Sparse Core Ops, SparseCore 0:
  298.0 75.7 all-gather.3
  375.4 37.3 all-gather.5
  414.3 35.7 all-gather.7
where the time goes:
time: 486 us; the launch traced here: 485 us
  waiting for transfers between devices  287 us (59%)
  blocking collectives  79.3 us (16%)
  local copies, waits for them, and re-layouts  42.8 us (9%)
  matrix products  24.1 us (5%)
  starting transfers between devices  19.7 us (4%)
  other arithmetic  19.1 us (4%)
  between operations  13.9 us (3%)
    all_to_all x1, waiting for transfers between devices, on_device(): lax.all_to_all(outbox.reshape(experts, capacity, width), ('fs', 'tp'), sp...  130 us
    all_to_all x1, waiting for transfers between devices, on_device(): lax.all_to_all(finished, ('fs', 'tp'), split_axis=0, concat_axis=0, tiled...  72.7 us
    all_gather x1, waiting for transfers between devices, on_device(): lax.all_gather(held_gate, 'fs', axis=0, tiled=True)  52.7 us
    all_to_all x1, blocking collectives, on_device(): lax.all_to_all(piece_gate[:, None], ('fs', 'tp'), split_axis=0, concat_ax...  31.1 us
    all_gather x1, blocking collectives, on_device(): lax.all_gather(tile_gate, 'tp', axis=1, tiled=True)  29.8 us
    all_to_all x1, waiting for transfers between devices, on_device(): lax.all_to_all(piece_up[:, None], ('fs', 'tp'), split_axis=0, concat_axis...  22.1 us
    dot_general x1, matrix products, expert_rows(): jnp.dot(hidden, w_down, preferred_element_type=jnp.float32)  12.9 us
    gather x1, local copies, waits for them, and re-layouts, on_device(): results = returned.reshape(experts * capacity, width)[target]  12.4 us
  transfers between devices with their start and end apart: 7, of which 5 were waited for; matrix products, arithmetic and copies ran while one was open for 12% of the time, Pallas kernels for 0%

commit v1 on v0

--- a/solution.py
+++ b/solution.py
@@ -1,10 +1,22 @@
+import functools
+import math
+
 import jax
 import jax.numpy as jnp
 from jax import lax
+from jax.experimental import pallas as pl
+from jax.experimental.pallas import tpu as pltpu
 from jax.sharding import PartitionSpec as P
 
 EPSILON = 1e-06
 route_scale = 2.5
+LANES = 128
+PACKED_ROWS = 16
+CORES = 2
+
+
+def ceil_to(value, unit):
+    return -(-value // unit) * unit
 
 
 def expert_rows(row_block, w_gate, w_up, w_down):
@@ -22,7 +34,7 @@
     return grid.reshape(1, fs_count * tile_rows, tp_count * tile_cols)
 
 
-def on_device(
+def exchange_plan(
     tokens,
     route_ids,
     route_scores,
@@ -111,6 +123,302 @@
     )
     mixed = (routed + shared_term).astype(jnp.bfloat16)
     return (mixed, served_gate, served_up, served_down, held_gate, held_up, held_down)
+
+
+def silu(value):
+    return value / (1.0 + jnp.exp(-value))
+
+
+def norm_kernel(experts, ids_ref, scores_ref, tokens_ref, out_ref):
+    rows, width = tokens_ref.shape
+    picks = ids_ref.shape[0]
+    extra = out_ref.shape[1] - width
+    widened = tokens_ref[...].astype(jnp.float32)
+    mean = jnp.mean(widened * widened, axis=1, keepdims=True)
+    out_ref[:, :width] = (widened * lax.rsqrt(mean + EPSILON)).astype(jnp.bfloat16)
+    scores = scores_ref[...]
+    weights = route_scale * scores / jnp.sum(scores, axis=0, keepdims=True)
+    place = lax.broadcasted_iota(jnp.int32, (experts, rows), 0)
+    dense = jnp.zeros((experts, rows), jnp.float32)
+    for k in range(picks):
+        dense = dense + jnp.where(ids_ref[k : k + 1, :] == place, weights[k : k + 1, :], 0.0)
+    first = dense.astype(jnp.bfloat16).astype(jnp.float32)
+    left = dense - first
+    second = left.astype(jnp.bfloat16).astype(jnp.float32)
+    third = left - second
+    blank = jnp.zeros((extra - 3 * experts, rows), jnp.float32)
+    stacked = jnp.concatenate([first, second, third, blank], axis=0)
+    out_ref[:, width:] = stacked.T.astype(jnp.bfloat16)
+
+
+def norm_rows(tokens, route_ids, route_scores, experts):
+    rows, width = tokens.shape
+    extra = ceil_to(3 * experts, LANES)
+    return pl.pallas_call(
+        functools.partial(norm_kernel, experts),
+        out_shape=jax.ShapeDtypeStruct((rows, width + extra), jnp.bfloat16),
+        name="norm_rows",
+    )(route_ids.T, route_scores.T, tokens)
+
+
+def pack_kernel(per_step, share, half_ref, gate_ref, up_ref, down_ref, sg_ref, su_ref, sd_ref, gain_ref, out_ref, tail_ref):
+    units = gate_ref.shape[1]
+    gain = gain_ref[...]
+    for j in range(per_step):
+        out_ref[j, :units] = (gate_ref[j] * gain).astype(jnp.bfloat16)
+        out_ref[j, units : 2 * units] = (up_ref[j] * gain).astype(jnp.bfloat16)
+        out_ref[j, 2 * units : 3 * units] = down_ref[j].astype(jnp.bfloat16)
+        rows = slice(j * share, (j + 1) * share)
+        tail_ref[...] = jnp.zeros(tail_ref.shape, jnp.float32)
+        tail_ref[:share] = sg_ref[rows] * gain
+        tail_ref[share : 2 * share] = su_ref[rows] * gain
+        tail_ref[2 * share : 3 * share] = sd_ref[rows]
+        out_ref[j, 3 * units :] = tail_ref[...].astype(jnp.bfloat16)
+
+
+def pack_tiles(half, halves, gate, up, down, sg, su, sd, gain):
+    experts, units, width = gate.shape
+    share = sg.shape[0] // experts
+    per_step = 8 // math.gcd(share, 8) * 2
+    part = width // halves
+    tail_rows = ceil_to(3 * share, PACKED_ROWS)
+    out_rows = 3 * units + tail_rows
+    tile = pl.BlockSpec((per_step, units, part), lambda i, h: (i, 0, h[0]))
+    strip = pl.BlockSpec((per_step * share, part), lambda i, h: (i, h[0]))
+    return pl.pallas_call(
+        functools.partial(pack_kernel, per_step, share),
+        grid_spec=pltpu.PrefetchScalarGridSpec(
+            num_scalar_prefetch=1,
+            grid=(experts // per_step,),
+            in_specs=[tile, tile, tile, strip, strip, strip, pl.BlockSpec((1, part), lambda i, h: (0, h[0]))],
+            out_specs=pl.BlockSpec((per_step, out_rows, part), lambda i, h: (i, 0, 0)),
+            scratch_shapes=[pltpu.VMEM((tail_rows, part), jnp.float32)],
+        ),
+        out_shape=jax.ShapeDtypeStruct((experts, out_rows, part), jnp.bfloat16),
+        name="pack_tiles",
+    )(half, gate, up, down, sg, su, sd, gain)
+
+
+def place_kernel(tp_count, units, halves, half_ref, *refs):
+    parts = refs[:halves]
+    first_ref, down_ref, shared_ref = refs[halves:]
+    part = parts[0].shape[2]
+    tail = parts[0].shape[1] - 3 * units
+    gate_rows = tp_count * units
+    for t in range(tp_count):
+        for h in range(halves):
+            if halves == 1:
+                piece = parts[0][t]
+            else:
+                piece = jnp.where(half_ref[0] == h, parts[0][t], parts[1][t])
+            cols = slice(h * part, (h + 1) * part)
+            far = slice((t * halves + h) * part, (t * halves + h + 1) * part)
+            first_ref[t * units : (t + 1) * units, cols] = piece[:units]
+            first_ref[gate_rows + t * units : gate_rows + (t + 1) * units, cols] = piece[units : 2 * units]
+            first_ref[2 * gate_rows + t * tail : 2 * gate_rows + (t + 1) * tail, cols] = piece[3 * units :]
+            down_ref[:, far] = piece[2 * units : 3 * units]
+            shared_ref[:, far] = piece[3 * units :]
+    used = 2 * gate_rows + tp_count * tail
+    if used < first_ref.shape[0]:
+        first_ref[used:, :] = jnp.zeros((first_ref.shape[0] - used, first_ref.shape[1]), jnp.bfloat16)
+
+
+def place_tiles(half, parts, fs_count, tp_count, units):
+    halves = len(parts)
+    rows, part = parts[0].shape[1], parts[0].shape[2]
+    tail = rows - 3 * units
+    width = halves * part
+    first_rows = 2 * tp_count * units + ceil_to(tp_count * tail, LANES)
+    block = pl.BlockSpec((tp_count, rows, part), lambda f, h: (f, 0, 0))
+    return pl.pallas_call(
+        functools.partial(place_kernel, tp_count, units, halves),
+        grid_spec=pltpu.PrefetchScalarGridSpec(
+            num_scalar_prefetch=1,
+            grid=(fs_count,),
+            in_specs=[block] * halves,
+            out_specs=[
+                pl.BlockSpec((first_rows, width), lambda f, h: (0, f)),
+                pl.BlockSpec((units, tp_count * width), lambda f, h: (f, 0)),
+                pl.BlockSpec((tail, tp_count * width), lambda f, h: (f, 0)),
+            ],
+        ),
+        out_shape=[
+            jax.ShapeDtypeStruct((first_rows, fs_count * width), jnp.bfloat16),
+            jax.ShapeDtypeStruct((fs_count * units, tp_count * width), jnp.bfloat16),
+            jax.ShapeDtypeStruct((fs_count * tail, tp_count * width), jnp.bfloat16),
+        ],
+        name="place_tiles",
+    )(half, *parts)
+
+
+def ffn_kernel(experts, share, tail, n_keep, own_ref, *refs):
+    blocks = refs[: 2 * n_keep]
+    first_ref, down_ref, shared_ref, keep_ref, give_ref = refs[2 * n_keep :]
+    rows = blocks[0].shape[0]
+    hidden_units, width = down_ref.shape
+    extra = blocks[0].shape[1] - width
+    tokens = jnp.concatenate([b[:, :width] for b in blocks], axis=0)
+    marks = jnp.concatenate([b[:, width:] for b in blocks], axis=0).astype(jnp.float32)
+    lane = lax.broadcasted_iota(jnp.int32, marks.shape, 1)
+    weight = jnp.sum(jnp.where(lax.rem(lane, experts) == own_ref[0], marks, 0.0), axis=1, keepdims=True)
+    nt = (((1,), (1,)), ((), ()))
+    into = lax.dot_general(tokens, first_ref[...], nt, preferred_element_type=jnp.float32)
+    gate = into[:, :hidden_units]
+    up = into[:, hidden_units : 2 * hidden_units]
+    hidden = (silu(gate) * up).astype(jnp.bfloat16)
+    strip = into[:, 2 * hidden_units :]
+    lanes = strip.shape[1]
+    place = lax.rem(lax.broadcasted_iota(jnp.int32, strip.shape, 1), tail)
+    mine = (place >= 2 * share) & (place < 3 * share)
+    near = jnp.where(mine, pltpu.roll(strip, 2 * share, 1), 0.0)
+    far = jnp.where(mine, pltpu.roll(strip, share, 1), 0.0)
+    shared_hidden = (silu(near) * far).astype(jnp.bfloat16)[:, : shared_ref.shape[0]]
+    out = weight * jnp.dot(hidden, down_ref[...], preferred_element_type=jnp.float32)
+    out = out + jnp.dot(shared_hidden, shared_ref[...], preferred_element_type=jnp.float32)
+    out = out.astype(jnp.bfloat16)
+    for j in range(n_keep):
+        keep_ref[j] = out[j * rows : (j + 1) * rows]
+        give_ref[j] = out[(n_keep + j) * rows : (n_keep + j + 1) * rows]
+
+
+def ffn(own, blocks, first, down, shared, experts, share, tail):
+    n_keep = len(blocks) // 2
+    rows, width = blocks[0].shape[0], down.shape[1]
+    shape = jax.ShapeDtypeStruct((n_keep, rows, width), jnp.bfloat16)
+    whole = pl.BlockSpec(memory_space=pltpu.VMEM)
+    return pl.pallas_call(
+        functools.partial(ffn_kernel, experts, share, tail, n_keep),
+        in_specs=[pl.BlockSpec(memory_space=pltpu.SMEM)] + [whole] * (len(blocks) + 3),
+        out_specs=[whole, whole],
+        out_shape=[shape, shape],
+        name="expert_ffn",
+    )(own, *blocks, first, down, shared)
+
+
+def held_kernel(order_ref, *refs):
+    tiles = refs[:-4]
+    gate_ref, up_ref, down_ref, stage_ref = refs[-4:]
+    units = tiles[0].shape[0] // 3
+    count = len(tiles)
+    width = tiles[0].shape[1]
+    for r in range(count):
+        spot = pl.multiple_of(order_ref[r] * units, units)
+        for m in range(3):
+            stage_ref[m, pl.ds(spot, units), :] = tiles[r][m * units : (m + 1) * units, :]
+    gate_ref[...] = stage_ref[0].T
+    up_ref[...] = stage_ref[1].T
+    for t in range(count):
+        down_ref[:, t * width : (t + 1) * width] = stage_ref[2, t * units : (t + 1) * units, :]
+
+
+def held_tiles(order, tiles):
+    count = len(tiles)
+    units, width = tiles[0].shape[0] // 3, tiles[0].shape[1]
+    whole = pl.BlockSpec(memory_space=pltpu.VMEM)
+    tall = jax.ShapeDtypeStruct((width, count * units), jnp.bfloat16)
+    return pl.pallas_call(
+        held_kernel,
+        in_specs=[pl.BlockSpec(memory_space=pltpu.SMEM)] + [whole] * count,
+        out_specs=[whole] * 3,
+        out_shape=[tall, tall, jax.ShapeDtypeStruct((units, count * width), jnp.bfloat16)],
+        scratch_shapes=[pltpu.VMEM((3, count * units, width), jnp.bfloat16)],
+        name="held_tiles",
+    )(order, *tiles)
+
+
+def gather_plan(
+    tokens,
+    route_ids,
+    route_scores,
+    norm_gain,
+    expert_gate,
+    expert_up,
+    expert_down,
+    shared_gate,
+    shared_up,
+    shared_down,
+):
+    groups = lax.axis_size("grp")
+    fs_count = lax.axis_size("fs")
+    tp_count = lax.axis_size("tp")
+    experts = fs_count * tp_count
+    columns = tp_count // CORES
+    halves = 2 if groups == 2 else 1
+    half = (lax.axis_index("grp") % halves).astype(jnp.int32)[None]
+    tp_index = lax.axis_index("tp").astype(jnp.int32)
+    own = (lax.axis_index("fs").astype(jnp.int32) * tp_count + tp_index)[None]
+
+    def along_fs(value, k):
+        return lax.ppermute(value, "fs", [(i, (i + k) % fs_count) for i in range(fs_count)])
+
+    def along_x(value, j):
+        return lax.ppermute(
+            value,
+            "tp",
+            [(i, (i // CORES + j) % columns * CORES + i % CORES) for i in range(tp_count)],
+        )
+
+    def across(value):
+        return lax.ppermute(value, "tp", [(i, i ^ 1) for i in range(tp_count)])
+
+    gain = norm_gain[None, :]
+    gate_t = jnp.transpose(expert_gate, (0, 2, 1))
+    up_t = jnp.transpose(expert_up, (0, 2, 1))
+    sg_t, su_t = shared_gate.T, shared_up.T
+    units = gate_t.shape[1]
+    share = sg_t.shape[0] // experts
+    packed = pack_tiles(half, halves, gate_t, up_t, expert_down, sg_t, su_t, shared_down, gain)
+    tail = packed.shape[1] - 3 * units
+    landed = lax.all_to_all(packed, ("fs", "tp"), split_axis=0, concat_axis=0, tiled=True)
+    parts = [landed]
+    if halves == 2:
+        parts.append(lax.ppermute(landed, "grp", [(0, 1), (1, 0)]))
+
+    normed = norm_rows(tokens, route_ids, route_scores, experts)
+    chunks = []
+    for k in range(fs_count):
+        block = normed if k == 0 else along_fs(normed, k)
+        column = [block] + [along_x(block, j) for j in range(1, columns)]
+        chunks.append(column + [across(b) for b in column])
+
+    first, served_down, shared_rows = place_tiles(half, parts, fs_count, tp_count, units)
+    gate_rows = tp_count * units
+    served_gate = first[:gate_rows].T
+    served_up = first[gate_rows : 2 * gate_rows].T
+
+    sums = []
+    for k in range(fs_count):
+        keep, give = ffn(own, chunks[k], first, served_down, shared_rows, experts, share, tail)
+        got = across(give)
+        total = keep[0].astype(jnp.float32) + got[0].astype(jnp.float32)
+        for j in range(1, columns):
+            step = (keep[j].astype(jnp.float32) + got[j].astype(jnp.float32)).astype(jnp.bfloat16)
+            total = total + along_x(step, -j).astype(jnp.float32)
+        if k > 0:
+            total = along_fs(total.astype(jnp.bfloat16), -k).astype(jnp.float32)
+        sums.append(total)
+    mixed = sums[0]
+    for total in sums[1:]:
+        mixed = mixed + total
+    mixed = mixed.astype(jnp.bfloat16)
+
+    tile = jnp.concatenate([gain * sg_t, gain * su_t, shared_down], axis=0).astype(jnp.bfloat16)
+    tiles, order = [], []
+    for j in range(columns):
+        tiles.append(tile if j == 0 else along_x(tile, j))
+        order.append(((tp_index // CORES - j) % columns) * CORES + tp_index % CORES)
+    for j in range(columns):
+        tiles.append(across(tiles[j]))
+        order.append(order[j] ^ 1)
+    held_gate, held_up, held_down = held_tiles(jnp.stack(order), tiles)
+    return (mixed, served_gate[None], served_up[None], served_down[None], held_gate, held_up, held_down)
+
+
+def on_device(tokens, route_ids, *others):
+    experts = lax.axis_size("fs") * lax.axis_size("tp")
+    if experts <= 2 * route_ids.shape[1]:
+        return gather_plan(tokens, route_ids, *others)
+    return exchange_plan(tokens, route_ids, *others)
 
 
 def solution(mesh):

time: 486 us -> 227 us (0.47)
  waiting for transfers between devices: 287 us -> 103 us
  blocking collectives: 79.3 us -> 0 us
  Pallas kernels: 0 us -> 41.1 us
  starting transfers between devices: 19.7 us -> 59.9 us
  local copies, waits for them, and re-layouts: 42.8 us -> 4.98 us
  matrix products: 24.1 us -> 0 us
  between operations: 13.9 us -> 0.82 us
    all_to_all x4 -> x1, waiting for transfers between devices: 234 us -> 46.4 us  [gather_plan(): lax.all_to_all(packed, ('fs', 'tp'), split_axis=0, concat_axis=0, tiled=T...]
    ppermute x0 -> x30, waiting for transfers between devices: none -> 57 us  [the longest x6 30.5 us: along_fs(): lax.ppermute(value, 'fs', [(i, (i + k) % fs_count) for i in range(fs_coun...]
    ppermute x0 -> x30, starting transfers between devices: none -> 53.3 us  [the longest x6 33.7 us: along_fs(): lax.ppermute(value, 'fs', [(i, (i + k) % fs_count) for i in range(fs_coun...]
    all_gather x3 -> x0, waiting for transfers between devices: 52.7 us -> none  [the longest x1 52.7 us: on_device(): lax.all_gather(held_gate, 'fs', axis=0, tiled=True)]
    all_gather x3 -> x0, blocking collectives: 48.2 us -> none  [the longest x1 29.8 us: on_device(): lax.all_gather(tile_gate, 'tp', axis=1, tiled=True)]
    pallas_call x0 -> x8, Pallas kernels: none -> 41.1 us  [the longest x4 28.3 us: ffn(): pl.pallas_call(functools.partial(ffn_kernel, experts, share, tail, n_keep...]
    all_to_all x1 -> x0, blocking collectives: 31.1 us -> none  [on_device(): lax.all_to_all(piece_gate[:, None], ('fs', 'tp'), split_axis=0, concat_ax...]
    dot_general x4 -> x0, matrix products: 24.1 us -> none  [the longest x1 12.9 us: expert_rows(): jnp.dot(hidden, w_down, preferred_element_type=jnp.float32)]
  transfers between devices with their start and end apart: 7 -> 31, of which waited for: 5 -> 8; matrix products, arithmetic and copies ran while one was open for 12% -> 6% of each run, Pallas kernels for 0% -> 17%
where the time goes in v1:
time: 227 us; the launch traced here: 224 us
  waiting for transfers between devices  103 us (45%)
  starting transfers between devices  59.9 us (26%)
  Pallas kernels  41.1 us (18%)
  other arithmetic  14.3 us (6%)
  local copies, waits for them, and re-layouts  4.98 us (2%)
    all_to_all x1, waiting for transfers between devices, gather_plan(): lax.all_to_all(packed, ('fs', 'tp'), split_axis=0, concat_axis=0, tiled=T...  46.4 us
    ppermute x6, starting transfers between devices, along_fs(): lax.ppermute(value, 'fs', [(i, (i + k) % fs_count) for i in range(fs_coun...  33.7 us
    ppermute x6, waiting for transfers between devices, along_fs(): lax.ppermute(value, 'fs', [(i, (i + k) % fs_count) for i in range(fs_coun...  30.5 us
    pallas_call x4, Pallas kernels, ffn(): pl.pallas_call(functools.partial(ffn_kernel, experts, share, tail, n_keep...  28.3 us
    ppermute x9, waiting for transfers between devices, along_x(): lax.ppermute(value, 'tp', [(i, (i // CORES + j) % columns * CORES + i % C...  26.4 us
    ppermute x9, starting transfers between devices, along_x(): lax.ppermute(value, 'tp', [(i, (i // CORES + j) % columns * CORES + i % C...  10.5 us
    ppermute x14, starting transfers between devices, across(): return lax.ppermute(value, 'tp', [(i, i ^ 1) for i in range(tp_count)])  7.78 us
    all_to_all x1, starting transfers between devices, gather_plan(): lax.all_to_all(packed, ('fs', 'tp'), split_axis=0, concat_axis=0, tiled=T...  6.67 us
  transfers between devices with their start and end apart: 31, of which 8 were waited for; matrix products, arithmetic and copies ran while one was open for 6% of the time, Pallas kernels for 17%

profile of v1, /device:TPU:11, one launch (start us, length us, event | category | flops | bytes accessed | tf_op | source)
XLA Modules:
  0.0 224.5 jit_solution(12312658239478403086)
XLA Ops:
  0.6 4.0 %pack_tiles.1 = bf16[16,208,256]{2,1,0:T(8,128)(2,1)} custom-call(s32[1]{0:T(128)} %bitcast.3.half_ref, f32[16,64,512]{2,1,0:T(8,128)} %bitcast.55, f32[16,64,512]{2,1,0:T(8,128)} %bitcast.56, f32[16,64,512]{2,1,0:T(8,128)} %down_ref.1, f32[64,512]{1,0:T(8,128)} %bitcast.57, f32[64,512]{1,0:T(8,128)} %bitcast.58, f32[64,512]{1,0:T(8,128)} %sd_ref.1, ...), custom_call_target="tpu_custom_call" | custom-call | tf_op jit(solution)/shard_map/pack_tiles/pallas_call | solution.py:188
  4.7 6.7 %all-to-all-start = ((bf16[16,208,256]{2,1,0:T(8,128)(2,1)}), bf16[16,208,256]{2,1,0:T(8,128)(2,1)S(1)}, u32[]{:S(2)}, u32[]{:S(2)}) async-start(bf16[16,208,256]{2,1,0:T(8,128)(2,1)} %pack_tiles.1), calls=%async_computation | async-start | bytes 3407872 | tf_op jit(solution)/shard_map/all_to_all | solution.py:372
  11.3 2.1 norm_rows.1.refs_0_
  13.7 46.4 %all-to-all-done.refs_0_ = bf16[16,208,256]{2,1,0:T(8,128)(2,1)S(1)} async-done(((bf16[16,208,256]{2,1,0:T(8,128)(2,1)}), bf16[16,208,256]{2,1,0:T(8,128)(2,1)S(1)}, u32[]{:S(2)}, u32[]{:S(2)}) %all-to-all-start) | async-done | bytes 1703968 | tf_op jit(solution)/shard_map/all_to_all | solution.py:372
  61.3 3.3 %collective-permute-start.13 = (bf16[128,2176]{1,0:T(8,128)(2,1)}, bf16[128,2176]{1,0:T(8,128)(2,1)}, u32[]{:S(2)}, u32[]{:S(2)}) collective-permute-start(bf16[128,2176]{1,0:T(8,128)(2,1)} %norm_rows.1.refs_0_), channel_id=1, source_target_pairs={{0,8},{4,12},{8,0},{12,4},{1,9},{5,13},{9,1},{13,5},{2,10},{6,14},... | collective-permute-start | bytes 1671176 | tf_op jit(solution)/shard_map/ppermute | solution.py:352
  68.1 16.5 %collective-permute-done.27.refs_1_ = bf16[192,512]{1,0:T(8,128)(2,1)} collective-permute-done((bf16[192,512]{1,0:T(8,128)(2,1)S(1)}, bf16[192,512]{1,0:T(8,128)(2,1)}, u32[]{:S(2)}, u32[]{:S(2)}) %collective-permute-start.27) | collective-permute-done | bytes 196640 | tf_op jit(solution)/shard_map/ppermute | solution.py:355
  89.0 8.3 %collective-permute-done.6.refs_0_ = bf16[128,2176]{1,0:T(8,128)(2,1)} collective-permute-done((bf16[128,2176]{1,0:T(8,128)(2,1)}, bf16[128,2176]{1,0:T(8,128)(2,1)}, u32[]{:S(2)}, u32[]{:S(2)}) %collective-permute-start.6) | collective-permute-done | bytes 557088 | tf_op jit(solution)/shard_map/ppermute | solution.py:352
  97.7 2.6 %collective-permute-start.7 = (bf16[128,2176]{1,0:T(8,128)(2,1)}, bf16[128,2176]{1,0:T(8,128)(2,1)}, u32[]{:S(2)}, u32[]{:S(2)}) collective-permute-start(bf16[128,2176]{1,0:T(8,128)(2,1)} %collective-permute-done.6.refs_0_), channel_id=1, source_target_pairs={{0,2},{1,3},{2,0},{3,1},{4,6},{5,7},{6,4},{7,5},{8,10},{9,11},{10,... | collective-permute-start | bytes 1671176 | tf_op jit(solution)/shard_map/ppermute | solution.py:355
  104.4 4.4 %place_tiles.1 = (bf16[640,2048]{1,0:T(8,128)(2,1)}, bf16[256,2048]{1,0:T(8,128)(2,1)}, bf16[64,2048]{1,0:T(8,128)(2,1)}) custom-call(s32[1]{0:T(128)} %bitcast.3.half_ref, bf16[16,208,256]{2,1,0:T(8,128)(2,1)} %copy-done.1, bf16[16,208,256]{2,1,0:T(8,128)(2,1)} %copy-done.3), custom_call_target="tpu_custom_call" | custom-call | tf_op jit(solution)/shard_map/place_tiles/pallas_call | solution.py:233
  108.8 7.1 %expert_ffn.7 = (bf16[2,128,2048]{2,1,0:T(8,128)(2,1)}, bf16[2,128,2048]{2,1,0:T(8,128)(2,1)}) custom-call(s32[1]{0:T(128)} %bitcast.own_ref, bf16[128,2176]{1,0:T(8,128)(2,1)} %collective-permute-done.20.refs_0_, bf16[128,2176]{1,0:T(8,128)(2,1)} %copy-done.13, bf16[128,2176]{1,0:T(8,128)(2,1)} %copy-done.14, bf16[128,2176]{1,0:T(8,128)(2,1)} %copy-done.15, ...), custom_call_target="tpu_custom_call" | custom-call | tf_op jit(solution)/shard_map/expert_ffn/pallas_call | solution.py:289
  116.8 7.0 %expert_ffn.6 = (bf16[2,128,2048]{2,1,0:T(8,128)(2,1)}, bf16[2,128,2048]{2,1,0:T(8,128)(2,1)}) custom-call(s32[1]{0:T(128)} %bitcast.own_ref, bf16[128,2176]{1,0:T(8,128)(2,1)} %collective-permute-done.13.refs_0_, bf16[128,2176]{1,0:T(8,128)(2,1)} %collective-permute-done.14.refs_1_, bf16[128,2176]{1,0:T(8,128)(2,1)} %collective-permute-done.15.refs_2_, ...), custom_call_target="tpu_custom_call" | custom-call | tf_op jit(solution)/shard_map/expert_ffn/pallas_call | solution.py:289
  127.1 7.1 %expert_ffn.5 = (bf16[2,128,2048]{2,1,0:T(8,128)(2,1)}, bf16[2,128,2048]{2,1,0:T(8,128)(2,1)}) custom-call(s32[1]{0:T(128)} %bitcast.own_ref, bf16[128,2176]{1,0:T(8,128)(2,1)} %collective-permute-done.6.refs_0_, bf16[128,2176]{1,0:T(8,128)(2,1)} %collective-permute-done.7.refs_1_, bf16[128,2176]{1,0:T(8,128)(2,1)} %collective-permute-done.8.refs_2_, ...), custom_call_target="tpu_custom_call" | custom-call | tf_op jit(solution)/shard_map/expert_ffn/pallas_call | solution.py:289
  135.4 2.3 %held_tiles.1 = (bf16[512,256]{1,0:T(8,128)(2,1)}, bf16[512,256]{1,0:T(8,128)(2,1)}, bf16[64,2048]{1,0:T(8,128)(2,1)}) custom-call(s32[4]{0:T(128)} %pad_add_fusion.order_ref, bf16[192,512]{1,0:T(8,128)(2,1)} %copy-done.10, bf16[192,512]{1,0:T(8,128)(2,1)} %collective-permute-done.27.refs_1_, bf16[192,512]{1,0:T(8,128)(2,1)} %copy-done.17, ...), custom_call_target="tpu_custom_call" | custom-call | tf_op jit(solution)/shard_map/held_tiles/pallas_call | solution.py:319
  137.6 7.1 %expert_ffn.4 = (bf16[2,128,2048]{2,1,0:T(8,128)(2,1)}, bf16[2,128,2048]{2,1,0:T(8,128)(2,1)}) custom-call(s32[1]{0:T(128)} %bitcast.own_ref, bf16[128,2176]{1,0:T(8,128)(2,1)} %norm_rows.1.refs_0_, bf16[128,2176]{1,0:T(8,128)(2,1)} %collective-permute-done.refs_1_, bf16[128,2176]{1,0:T(8,128)(2,1)} %collective-permute-done.1.refs_2_, ...), custom_call_target="tpu_custom_call" | custom-call | tf_op jit(solution)/shard_map/expert_ffn/pallas_call | solution.py:289
  152.9 5.1 %collective-permute-done.25 = bf16[128,2048]{1,0:T(8,128)(2,1)S(1)} collective-permute-done((bf16[128,2048]{1,0:T(8,128)(2,1)S(1)}, bf16[128,2048]{1,0:T(8,128)(2,1)S(1)}, u32[]{:S(2)}, u32[]{:S(2)}) %collective-permute-start.25) | collective-permute-done | bytes 524320 | tf_op jit(solution)/shard_map/ppermute | solution.py:355
  159.1 12.2 %collective-permute-start.26 = (bf16[128,2048]{1,0:T(8,128)(2,1)}, bf16[128,2048]{1,0:T(8,128)(2,1)}, u32[]{:S(2)}, u32[]{:S(2)}) collective-permute-start(bf16[128,2048]{1,0:T(8,128)(2,1)} %fusion), channel_id=1, source_target_pairs={{0,4},{4,8},{8,12},{12,0},{1,5},{5,9},{9,13},{13,1},{2,6},{6,10},{... | collective-permute-start | bytes 1572872 | tf_op jit(solution)/shard_map/ppermute | solution.py:352
  171.2 2.1 fusion.1
  173.3 4.0 %collective-permute-start.19 = (bf16[128,2048]{1,0:T(8,128)(2,1)}, bf16[128,2048]{1,0:T(8,128)(2,1)}, u32[]{:S(2)}, u32[]{:S(2)}) collective-permute-start(bf16[128,2048]{1,0:T(8,128)(2,1)} %fusion.1), channel_id=1, source_target_pairs={{0,8},{4,12},{8,0},{12,4},{1,9},{5,13},{9,1},{13,5},{2,10},{6,14},... | collective-permute-start | bytes 1572872 | tf_op jit(solution)/shard_map/ppermute | solution.py:352
  177.3 3.3 %collective-permute-done.11 = bf16[128,2048]{1,0:T(8,128)(2,1)S(1)} collective-permute-done((bf16[128,2048]{1,0:T(8,128)(2,1)S(1)}, bf16[128,2048]{1,0:T(8,128)(2,1)S(1)}, u32[]{:S(2)}, u32[]{:S(2)}) %collective-permute-start.11) | collective-permute-done | bytes 524320 | tf_op jit(solution)/shard_map/ppermute | solution.py:355
  180.6 2.1 fusion.2
  182.7 14.0 %collective-permute-start.12 = (bf16[128,2048]{1,0:T(8,128)(2,1)}, bf16[128,2048]{1,0:T(8,128)(2,1)}, u32[]{:S(2)}, u32[]{:S(2)}) collective-permute-start(bf16[128,2048]{1,0:T(8,128)(2,1)} %fusion.2), channel_id=1, source_target_pairs={{0,12},{4,0},{8,4},{12,8},{1,13},{5,1},{9,5},{13,9},{2,14},{6,2},{... | collective-permute-start | bytes 1572872 | tf_op jit(solution)/shard_map/ppermute | solution.py:352
  199.4 14.9 %collective-permute-done.19 = bf16[128,2048]{1,0:T(8,128)(2,1)} collective-permute-done((bf16[128,2048]{1,0:T(8,128)(2,1)}, bf16[128,2048]{1,0:T(8,128)(2,1)}, u32[]{:S(2)}, u32[]{:S(2)}) %collective-permute-start.19) | collective-permute-done | bytes 524320 | tf_op jit(solution)/shard_map/ppermute | solution.py:352
  214.3 7.3 %collective-permute-done.12 = bf16[128,2048]{1,0:T(8,128)(2,1)} collective-permute-done((bf16[128,2048]{1,0:T(8,128)(2,1)}, bf16[128,2048]{1,0:T(8,128)(2,1)}, u32[]{:S(2)}, u32[]{:S(2)}) %collective-permute-start.12) | collective-permute-done | bytes 524320 | tf_op jit(solution)/shard_map/ppermute | solution.py:352
  221.7 2.8 %fusion.6 = bf16[128,2048]{1,0:T(8,128)(2,1)} fusion(bf16[128,2048]{1,0:T(8,128)(2,1)} %collective-permute-done.26, bf16[128,2048]{1,0:T(8,128)(2,1)} %collective-permute-done.19, bf16[128,2048]{1,0:T(8,128)(2,1)} %collective-permute-done.12, bf16[128,2048]{1,0:T(8,128)(2,1)} %collective-permute-done.5, bf16[2,128,2048]{2,1,0:T(8,128)(2,1)S(1)} %copy-done.6, ...), kind=kLoop, calls=%fused_computation.10 | loop fusion | flops 3145728 | bytes 3670016 | tf_op jit(solution)/shard_map/convert_element_type | solution.py:403
  (101 shorter events, 31.1 us)
Async XLA Ops:
  4.7 55.4 %all-to-all-start = ((bf16[16,208,256]{2,1,0:T(8,128)(2,1)}), bf16[16,208,256]{2,1,0:T(8,128)(2,1)S(1)}, u32[]{:S(2)}, u32[]{:S(2)}) async-start(bf16[16,208,256]{2,1,0:T(8,128)(2,1)} %pack_tiles.1), calls=%async_computation | async-start | bytes 3407872 | tf_op jit(solution)/shard_map/all_to_all | solution.py:372
  13.4 53.1 %collective-permute-start.20 = (bf16[128,2176]{1,0:T(8,128)(2,1)}, bf16[128,2176]{1,0:T(8,128)(2,1)}, u32[]{:S(2)}, u32[]{:S(2)}) collective-permute-start(bf16[128,2176]{1,0:T(8,128)(2,1)} %norm_rows.1.refs_0_), channel_id=1, source_target_pairs={{0,12},{4,0},{8,4},{12,8},{1,13},{5,1},{9,5},{13,9},{2,14},{6,2},{... | collective-permute-start | bytes 1671176 | tf_op jit(solution)/shard_map/ppermute | solution.py:352
  60.1 43.0 %collective-permute-start.3 = (bf16[16,208,256]{2,1,0:T(8,128)(2,1)S(1)}, bf16[16,208,256]{2,1,0:T(8,128)(2,1)S(1)}, u32[]{:S(2)}, u32[]{:S(2)}) collective-permute-start(bf16[16,208,256]{2,1,0:T(8,128)(2,1)S(1)} %all-to-all-done.refs_0_), channel_id=1, source_target_pairs={{0,16},{16,0},{1,17},{17,1},{2,18},{18,2},{3,19},{19,3},{4,20},{20... | collective-permute-start | bytes 5111816 | tf_op jit(solution)/shard_map/ppermute | solution.py:375
  61.3 24.8 %collective-permute-start.13 = (bf16[128,2176]{1,0:T(8,128)(2,1)}, bf16[128,2176]{1,0:T(8,128)(2,1)}, u32[]{:S(2)}, u32[]{:S(2)}) collective-permute-start(bf16[128,2176]{1,0:T(8,128)(2,1)} %norm_rows.1.refs_0_), channel_id=1, source_target_pairs={{0,8},{4,12},{8,0},{12,4},{1,9},{5,13},{9,1},{13,5},{2,10},{6,14},... | collective-permute-start | bytes 1671176 | tf_op jit(solution)/shard_map/ppermute | solution.py:352
  66.5 21.2 %collective-permute-start.21 = (bf16[128,2176]{1,0:T(8,128)(2,1)}, bf16[128,2176]{1,0:T(8,128)(2,1)S(1)}, u32[]{:S(2)}, u32[]{:S(2)}) collective-permute-start(bf16[128,2176]{1,0:T(8,128)(2,1)} %collective-permute-done.20.refs_0_), channel_id=1, source_target_pairs={{0,2},{1,3},{2,0},{3,1},{4,6},{5,7},{6,4},{7,5},{8,10},{9,11},{10,... | collective-permute-start | bytes 1671176 | tf_op jit(solution)/shard_map/ppermute | solution.py:355
  66.6 18.0 %collective-permute-start.27 = (bf16[192,512]{1,0:T(8,128)(2,1)S(1)}, bf16[192,512]{1,0:T(8,128)(2,1)}, u32[]{:S(2)}, u32[]{:S(2)}) collective-permute-start(bf16[192,512]{1,0:T(8,128)(2,1)S(1)} %pad_maximum_fusion.refs_0_), channel_id=1, source_target_pairs={{0,2},{1,3},{2,0},{3,1},{4,6},{5,7},{6,4},{7,5},{8,10},{9,11},{10,... | collective-permute-start | bytes 589832 | tf_op jit(solution)/shard_map/ppermute | solution.py:355
  68.1 29.1 %collective-permute-start.6 = (bf16[128,2176]{1,0:T(8,128)(2,1)}, bf16[128,2176]{1,0:T(8,128)(2,1)}, u32[]{:S(2)}, u32[]{:S(2)}) collective-permute-start(bf16[128,2176]{1,0:T(8,128)(2,1)} %norm_rows.1.refs_0_), channel_id=1, source_target_pairs={{0,4},{4,8},{8,12},{12,0},{1,5},{5,9},{9,13},{13,1},{2,6},{6,10},{... | collective-permute-start | bytes 1671176 | tf_op jit(solution)/shard_map/ppermute | solution.py:352
  86.1 14.2 %collective-permute-start.14 = (bf16[128,2176]{1,0:T(8,128)(2,1)}, bf16[128,2176]{1,0:T(8,128)(2,1)}, u32[]{:S(2)}, u32[]{:S(2)}) collective-permute-start(bf16[128,2176]{1,0:T(8,128)(2,1)} %collective-permute-done.13.refs_0_), channel_id=1, source_target_pairs={{0,2},{1,3},{2,0},{3,1},{4,6},{5,7},{6,4},{7,5},{8,10},{9,11},{10,... | collective-permute-start | bytes 1671176 | tf_op jit(solution)/shard_map/ppermute | solution.py:355
  87.7 13.9 %collective-permute-start.23 = (bf16[128,2176]{1,0:T(8,128)(2,1)S(1)}, bf16[128,2176]{1,0:T(8,128)(2,1)S(1)}, u32[]{:S(2)}, u32[]{:S(2)}) collective-permute-start(bf16[128,2176]{1,0:T(8,128)(2,1)S(1)} %collective-permute-done.21.refs_1_), channel_id=1, source_target_pairs={{0,1},{1,0},{2,3},{3,2},{4,5},{5,4},{6,7},{7,6},{8,9},{9,8},{10,11... | collective-permute-start | bytes 1671176 | tf_op jit(solution)/shard_map/ppermute | solution.py:362
  97.2 18.6 %collective-permute-start.15 = (bf16[128,2176]{1,0:T(8,128)(2,1)}, bf16[128,2176]{1,0:T(8,128)(2,1)}, u32[]{:S(2)}, u32[]{:S(2)}) collective-permute-start(bf16[128,2176]{1,0:T(8,128)(2,1)} %collective-permute-done.13.refs_0_), channel_id=1, source_target_pairs={{0,1},{1,0},{2,3},{3,2},{4,5},{5,4},{6,7},{7,6},{8,9},{9,8},{10,11... | collective-permute-start | bytes 1671176 | tf_op jit(solution)/shard_map/ppermute | solution.py:362
  97.7 18.5 %collective-permute-start.7 = (bf16[128,2176]{1,0:T(8,128)(2,1)}, bf16[128,2176]{1,0:T(8,128)(2,1)}, u32[]{:S(2)}, u32[]{:S(2)}) collective-permute-start(bf16[128,2176]{1,0:T(8,128)(2,1)} %collective-permute-done.6.refs_0_), channel_id=1, source_target_pairs={{0,2},{1,3},{2,0},{3,1},{4,6},{5,7},{6,4},{7,5},{8,10},{9,11},{10,... | collective-permute-start | bytes 1671176 | tf_op jit(solution)/shard_map/ppermute | solution.py:355
  100.3 16.1 %collective-permute-start.16 = (bf16[128,2176]{1,0:T(8,128)(2,1)}, bf16[128,2176]{1,0:T(8,128)(2,1)}, u32[]{:S(2)}, u32[]{:S(2)}) collective-permute-start(bf16[128,2176]{1,0:T(8,128)(2,1)} %collective-permute-done.14.refs_1_), channel_id=1, source_target_pairs={{0,1},{1,0},{2,3},{3,2},{4,5},{5,4},{6,7},{7,6},{8,9},{9,8},{10,11... | collective-permute-start | bytes 1671176 | tf_op jit(solution)/shard_map/ppermute | solution.py:362
  101.6 23.9 %collective-permute-start = (bf16[128,2176]{1,0:T(8,128)(2,1)}, bf16[128,2176]{1,0:T(8,128)(2,1)}, u32[]{:S(2)}, u32[]{:S(2)}) collective-permute-start(bf16[128,2176]{1,0:T(8,128)(2,1)} %norm_rows.1.refs_0_), channel_id=1, source_target_pairs={{0,2},{1,3},{2,0},{3,1},{4,6},{5,7},{6,4},{7,5},{8,10},{9,11},{10,... | collective-permute-start | bytes 1671176 | tf_op jit(solution)/shard_map/ppermute | solution.py:355
  103.1 23.1 %collective-permute-start.8 = (bf16[128,2176]{1,0:T(8,128)(2,1)}, bf16[128,2176]{1,0:T(8,128)(2,1)}, u32[]{:S(2)}, u32[]{:S(2)}) collective-permute-start(bf16[128,2176]{1,0:T(8,128)(2,1)} %collective-permute-done.6.refs_0_), channel_id=1, source_target_pairs={{0,1},{1,0},{2,3},{3,2},{4,5},{5,4},{6,7},{7,6},{8,9},{9,8},{10,11... | collective-permute-start | bytes 1671176 | tf_op jit(solution)/shard_map/ppermute | solution.py:362
  115.8 28.9 %collective-permute-start.24 = (bf16[2,128,2048]{2,1,0:T(8,128)(2,1)}, bf16[2,128,2048]{2,1,0:T(8,128)(2,1)S(1)}, u32[]{:S(2)}, u32[]{:S(2)}) collective-permute-start(bf16[2,128,2048]{2,1,0:T(8,128)(2,1)} %get-tuple-element.31), channel_id=1, source_target_pairs={{0,1},{1,0},{2,3},{3,2},{4,5},{5,4},{6,7},{7,6},{8,9},{9,8},{10,11... | collective-permute-start | bytes 3145736 | tf_op jit(solution)/shard_map/ppermute | solution.py:362
  123.8 22.7 %collective-permute-start.17 = (bf16[2,128,2048]{2,1,0:T(8,128)(2,1)}, bf16[2,128,2048]{2,1,0:T(8,128)(2,1)}, u32[]{:S(2)}, u32[]{:S(2)}) collective-permute-start(bf16[2,128,2048]{2,1,0:T(8,128)(2,1)} %get-tuple-element.29), channel_id=1, source_target_pairs={{0,1},{1,0},{2,3},{3,2},{4,5},{5,4},{6,7},{7,6},{8,9},{9,8},{10,11... | collective-permute-start | bytes 3145736 | tf_op jit(solution)/shard_map/ppermute | solution.py:362
  134.2 13.9 %collective-permute-start.10 = (bf16[2,128,2048]{2,1,0:T(8,128)(2,1)}, bf16[2,128,2048]{2,1,0:T(8,128)(2,1)}, u32[]{:S(2)}, u32[]{:S(2)}) collective-permute-start(bf16[2,128,2048]{2,1,0:T(8,128)(2,1)} %get-tuple-element.27), channel_id=1, source_target_pairs={{0,1},{1,0},{2,3},{3,2},{4,5},{5,4},{6,7},{7,6},{8,9},{9,8},{10,11... | collective-permute-start | bytes 3145736 | tf_op jit(solution)/shard_map/ppermute | solution.py:362
  144.9 13.1 %collective-permute-start.25 = (bf16[128,2048]{1,0:T(8,128)(2,1)S(1)}, bf16[128,2048]{1,0:T(8,128)(2,1)S(1)}, u32[]{:S(2)}, u32[]{:S(2)}) collective-permute-start(bf16[128,2048]{1,0:T(8,128)(2,1)S(1)} %fusion.10), channel_id=1, source_target_pairs={{0,2},{1,3},{2,0},{3,1},{4,6},{5,7},{6,4},{7,5},{8,10},{9,11},{10,... | collective-permute-start | bytes 1572872 | tf_op jit(solution)/shard_map/ppermute | solution.py:355
  147.8 23.4 %collective-permute-start.18 = (bf16[128,2048]{1,0:T(8,128)(2,1)S(1)}, bf16[128,2048]{1,0:T(8,128)(2,1)S(1)}, u32[]{:S(2)}, u32[]{:S(2)}) collective-permute-start(bf16[128,2048]{1,0:T(8,128)(2,1)S(1)} %fusion.9), channel_id=1, source_target_pairs={{0,2},{1,3},{2,0},{3,1},{4,6},{5,7},{6,4},{7,5},{8,10},{9,11},{10,... | collective-permute-start | bytes 1572872 | tf_op jit(solution)/shard_map/ppermute | solution.py:355
  149.4 31.2 %collective-permute-start.11 = (bf16[128,2048]{1,0:T(8,128)(2,1)S(1)}, bf16[128,2048]{1,0:T(8,128)(2,1)S(1)}, u32[]{:S(2)}, u32[]{:S(2)}) collective-permute-start(bf16[128,2048]{1,0:T(8,128)(2,1)S(1)} %fusion.8), channel_id=1, source_target_pairs={{0,2},{1,3},{2,0},{3,1},{4,6},{5,7},{6,4},{7,5},{8,10},{9,11},{10,... | collective-permute-start | bytes 1572872 | tf_op jit(solution)/shard_map/ppermute | solution.py:355
  152.8 46.7 %collective-permute-start.5 = (bf16[128,2048]{1,0:T(8,128)(2,1)}, bf16[128,2048]{1,0:T(8,128)(2,1)}, u32[]{:S(2)}, u32[]{:S(2)}) collective-permute-start(bf16[128,2048]{1,0:T(8,128)(2,1)} %fusion.7), channel_id=1, source_target_pairs={{0,2},{1,3},{2,0},{3,1},{4,6},{5,7},{6,4},{7,5},{8,10},{9,11},{10,... | collective-permute-start | bytes 1572872 | tf_op jit(solution)/shard_map/ppermute | solution.py:355
  159.1 40.3 %collective-permute-start.26 = (bf16[128,2048]{1,0:T(8,128)(2,1)}, bf16[128,2048]{1,0:T(8,128)(2,1)}, u32[]{:S(2)}, u32[]{:S(2)}) collective-permute-start(bf16[128,2048]{1,0:T(8,128)(2,1)} %fusion), channel_id=1, source_target_pairs={{0,4},{4,8},{8,12},{12,0},{1,5},{5,9},{9,13},{13,1},{2,6},{6,10},{... | collective-permute-start | bytes 1572872 | tf_op jit(solution)/shard_map/ppermute | solution.py:352
  173.3 41.0 %collective-permute-start.19 = (bf16[128,2048]{1,0:T(8,128)(2,1)}, bf16[128,2048]{1,0:T(8,128)(2,1)}, u32[]{:S(2)}, u32[]{:S(2)}) collective-permute-start(bf16[128,2048]{1,0:T(8,128)(2,1)} %fusion.1), channel_id=1, source_target_pairs={{0,8},{4,12},{8,0},{12,4},{1,9},{5,13},{9,1},{13,5},{2,10},{6,14},... | collective-permute-start | bytes 1572872 | tf_op jit(solution)/shard_map/ppermute | solution.py:352
  182.7 39.0 %collective-permute-start.12 = (bf16[128,2048]{1,0:T(8,128)(2,1)}, bf16[128,2048]{1,0:T(8,128)(2,1)}, u32[]{:S(2)}, u32[]{:S(2)}) collective-permute-start(bf16[128,2048]{1,0:T(8,128)(2,1)} %fusion.2), channel_id=1, source_target_pairs={{0,12},{4,0},{8,4},{12,8},{1,13},{5,1},{9,5},{13,9},{2,14},{6,2},{... | collective-permute-start | bytes 1572872 | tf_op jit(solution)/shard_map/ppermute | solution.py:352
  (27 other events, 425.5 us)

commit v2 on v0

--- a/solution.py
+++ b/solution.py
@@ -1,10 +1,25 @@
+import functools
+
 import jax
 import jax.numpy as jnp
 from jax import lax
+from jax.experimental import pallas as pl
+from jax.experimental.pallas import tpu as pltpu
 from jax.sharding import PartitionSpec as P
+
 
 EPSILON = 1e-06
 route_scale = 2.5
+LANES = 128
+PACKED_ROWS = 16
+CORES = 2
+IN_VMEM = pl.BlockSpec(memory_space=pltpu.VMEM)
+IN_SMEM = pl.BlockSpec(memory_space=pltpu.SMEM)
+SMALL_GRANT = pltpu.CompilerParams(vmem_limit_bytes=16 * 1024 * 1024)
+
+
+def ceil_to(value, unit):
+    return -(-value // unit) * unit
 
 
 def expert_rows(row_block, w_gate, w_up, w_down):
@@ -22,7 +37,7 @@
     return grid.reshape(1, fs_count * tile_rows, tp_count * tile_cols)
 
 
-def on_device(
+def exchange_plan(
     tokens,
     route_ids,
     route_scores,
@@ -111,6 +126,389 @@
     )
     mixed = (routed + shared_term).astype(jnp.bfloat16)
     return (mixed, served_gate, served_up, served_down, held_gate, held_up, held_down)
+
+
+def silu(value):
+    return value / (1.0 + jnp.exp(-value))
+
+
+def norm_kernel(experts, tiles, half_ref, ids_ref, scores_ref, tokens_ref, low_ref, high_ref):
+    rows, width = tokens_ref.shape
+    picks = ids_ref.shape[0]
+    extra = low_ref.shape[1] - width
+    widened = tokens_ref[...].astype(jnp.float32)
+    mean = jnp.mean(widened * widened, axis=1, keepdims=True)
+    normed = (widened * lax.rsqrt(mean + EPSILON)).astype(jnp.bfloat16)
+    scores = scores_ref[...]
+    weights = route_scale * scores / jnp.sum(scores, axis=0, keepdims=True)
+    place = lax.broadcasted_iota(jnp.int32, (experts, rows), 0)
+    dense = jnp.zeros((experts, rows), jnp.float32)
+    for k in range(picks):
+        dense = dense + jnp.where(ids_ref[k : k + 1, :] == place, weights[k : k + 1, :], 0.0)
+    first = dense.astype(jnp.bfloat16).astype(jnp.float32)
+    left = dense - first
+    second = left.astype(jnp.bfloat16).astype(jnp.float32)
+    third = left - second
+    blank = jnp.zeros((extra - 3 * experts, rows), jnp.float32)
+    marks = jnp.concatenate([first, second, third, blank], axis=0).T.astype(jnp.bfloat16)
+    part = width // tiles // 2
+    swap = half_ref[0] != 0
+    for n, ref in enumerate((low_ref, high_ref)):
+        mine = slice(n * (rows // 2), (n + 1) * (rows // 2))
+        for i in range(tiles):
+            left_cols = normed[mine, (2 * i) * part : (2 * i + 1) * part]
+            right_cols = normed[mine, (2 * i + 1) * part : (2 * i + 2) * part]
+            ref[:, i * part : (i + 1) * part] = jnp.where(swap, right_cols, left_cols)
+            far = slice(width // 2 + i * part, width // 2 + (i + 1) * part)
+            ref[:, far] = jnp.where(swap, left_cols, right_cols)
+        ref[:, width:] = marks[mine]
+
+
+def norm_rows(half, tokens, route_ids, route_scores, experts, tiles):
+    rows, width = tokens.shape
+    extra = ceil_to(3 * experts, LANES)
+    shape = jax.ShapeDtypeStruct((rows // 2, width + extra), jnp.bfloat16)
+    return pl.pallas_call(
+        functools.partial(norm_kernel, experts, tiles),
+        in_specs=[IN_SMEM] + [IN_VMEM] * 3,
+        out_specs=[IN_VMEM] * 2,
+        out_shape=[shape, shape],
+        compiler_params=SMALL_GRANT,
+        name="norm_rows",
+    )(half, route_ids.T, route_scores.T, tokens)
+
+
+def pack_kernel(per_step, share, half_ref, gate_ref, up_ref, down_ref, sg_ref, su_ref, sd_ref, gain_ref, out_ref, tail_ref):
+    units = gate_ref.shape[1]
+    gain = gain_ref[...]
+    for j in range(per_step):
+        out_ref[j, :units] = (gate_ref[j] * gain).astype(jnp.bfloat16)
+        out_ref[j, units : 2 * units] = (up_ref[j] * gain).astype(jnp.bfloat16)
+        out_ref[j, 2 * units : 3 * units] = down_ref[j].astype(jnp.bfloat16)
+        rows = slice(j * share, (j + 1) * share)
+        tail_ref[...] = jnp.zeros(tail_ref.shape, jnp.float32)
+        tail_ref[:share] = sg_ref[rows] * gain
+        tail_ref[share : 2 * share] = su_ref[rows] * gain
+        tail_ref[2 * share : 3 * share] = sd_ref[rows]
+        out_ref[j, 3 * units :] = tail_ref[...].astype(jnp.bfloat16)
+
+
+def pack_tiles(half, gate, up, down, sg, su, sd, gain):
+    experts, units, width = gate.shape
+    share = sg.shape[0] // experts
+    per_step = experts // 4
+    part = width // 2
+    tail_rows = ceil_to(3 * share, PACKED_ROWS)
+    out_rows = 3 * units + tail_rows
+    tile = pl.BlockSpec((per_step, units, part), lambda i, h: (i, 0, h[0]))
+    strip = pl.BlockSpec((per_step * share, part), lambda i, h: (i, h[0]))
+    return pl.pallas_call(
+        functools.partial(pack_kernel, per_step, share),
+        grid_spec=pltpu.PrefetchScalarGridSpec(
+            num_scalar_prefetch=1,
+            grid=(experts // per_step,),
+            in_specs=[tile, tile, tile, strip, strip, strip, pl.BlockSpec((1, part), lambda i, h: (0, h[0]))],
+            out_specs=pl.BlockSpec((per_step, out_rows, part), lambda i, h: (i, 0, 0)),
+            scratch_shapes=[pltpu.VMEM((tail_rows, part), jnp.float32)],
+        ),
+        out_shape=jax.ShapeDtypeStruct((experts, out_rows, part), jnp.bfloat16),
+        compiler_params=SMALL_GRANT,
+        name="pack_tiles",
+    )(half, gate, up, down, sg, su, sd, gain)
+
+
+def place_kernel(fs_count, tp_count, units, in_ref, out_ref):
+    part = in_ref.shape[2]
+    tail = in_ref.shape[1] - 3 * units
+    gate_rows = tp_count * units
+    strip_at = 2 * gate_rows
+    down_at = strip_at + tp_count * tail
+    shared_at = down_at + fs_count * units
+    for f in range(fs_count):
+        for t in range(tp_count):
+            src = f * tp_count + t
+            cols = slice(f * part, (f + 1) * part)
+            out_ref[t * units : (t + 1) * units, cols] = in_ref[src, :units]
+            out_ref[gate_rows + t * units : gate_rows + (t + 1) * units, cols] = in_ref[src, units : 2 * units]
+            last = in_ref[src, 3 * units :]
+            out_ref[strip_at + t * tail : strip_at + (t + 1) * tail, cols] = last
+            cols = slice(t * part, (t + 1) * part)
+            out_ref[down_at + f * units : down_at + (f + 1) * units, cols] = in_ref[src, 2 * units : 3 * units]
+            out_ref[shared_at + f * tail : shared_at + (f + 1) * tail, cols] = last
+
+
+def place_tiles(landed, fs_count, tp_count, units):
+    rows, part = landed.shape[1:]
+    tail = rows - 3 * units
+    out_rows = 2 * tp_count * units + tp_count * tail + fs_count * (units + tail)
+    return pl.pallas_call(
+        functools.partial(place_kernel, fs_count, tp_count, units),
+        in_specs=[IN_VMEM],
+        out_specs=IN_VMEM,
+        out_shape=jax.ShapeDtypeStruct((out_rows, fs_count * part), jnp.bfloat16),
+        compiler_params=SMALL_GRANT,
+        name="place_tiles",
+    )(landed)
+
+
+def ffn_kernel(experts, gate_rows, strip_rows, down_rows, share, tail, count, own_ref, *refs):
+    blocks = refs[:count]
+    own_low, peer_low, own_high, peer_high = refs[count : count + 4]
+    outs = refs[count + 4 :]
+    rows, part = blocks[0].shape[0], own_low.shape[1]
+    width = 2 * part
+    low = jnp.concatenate([b[:, :part] for b in blocks], axis=0)
+    high = jnp.concatenate([b[:, part:width] for b in blocks], axis=0)
+    marks = jnp.concatenate([b[:, width:] for b in blocks], axis=0).astype(jnp.float32)
+    lane = lax.rem(lax.broadcasted_iota(jnp.int32, marks.shape, 1), experts)
+    strip_at = 2 * gate_rows
+    down_at = strip_at + strip_rows
+    shared_at = down_at + down_rows
+
+    def into(a, b):
+        nt = (((1,), (1,)), ((), ()))
+        return lax.dot_general(a, b, nt, preferred_element_type=jnp.float32)
+
+    def onto(a, b):
+        return jnp.dot(a, b, preferred_element_type=jnp.float32)
+
+    hidden = []
+    for n, (near, far) in enumerate(((own_low, own_high), (peer_low, peer_high))):
+        weight = jnp.sum(jnp.where(lane == own_ref[n], marks, 0.0), axis=1, keepdims=True)
+        both = into(low, near[:strip_at]) + into(high, far[:strip_at])
+        hidden.append((weight * silu(both[:, :gate_rows]) * both[:, gate_rows:]).astype(jnp.bfloat16))
+    near = jnp.concatenate([own_low[strip_at:down_at], peer_low[strip_at:down_at]], axis=0)
+    far = jnp.concatenate([own_high[strip_at:down_at], peer_high[strip_at:down_at]], axis=0)
+    strip = into(low, near) + into(high, far)
+    place = lax.rem(lax.broadcasted_iota(jnp.int32, strip.shape, 1), tail)
+    mine = (place >= 2 * share) & (place < 3 * share)
+    gate = jnp.where(mine, pltpu.roll(strip, 2 * share, 1), 0.0)
+    up = jnp.where(mine, pltpu.roll(strip, share, 1), 0.0)
+    shared_hidden = (silu(gate) * up).astype(jnp.bfloat16)
+    for n, (own, peer) in enumerate(((own_low, peer_low), (own_high, peer_high))):
+        shared = jnp.concatenate([own[shared_at:], peer[shared_at:]], axis=0)
+        total = onto(hidden[0], own[down_at:shared_at]) + onto(hidden[1], peer[down_at:shared_at])
+        total = (total + onto(shared_hidden, shared)).astype(jnp.bfloat16)
+        for j in range(count):
+            outs[j][:, n * part : (n + 1) * part] = total[j * rows : (j + 1) * rows]
+
+
+def ffn(own, blocks, mats, experts, sizes):
+    rows, width = blocks[0].shape[0], 2 * mats[0].shape[1]
+    shape = jax.ShapeDtypeStruct((rows, width), jnp.bfloat16)
+    return pl.pallas_call(
+        functools.partial(ffn_kernel, experts, *sizes, len(blocks)),
+        in_specs=[IN_SMEM] + [IN_VMEM] * (len(blocks) + 4),
+        out_specs=[IN_VMEM] * len(blocks),
+        out_shape=[shape] * len(blocks),
+        compiler_params=SMALL_GRANT,
+        name="expert_ffn",
+    )(own, *blocks, *mats)
+
+
+def finish_kernel(tiles, half_ref, *refs):
+    out_ref = refs[-1]
+    rows, width = out_ref.shape
+    part = width // tiles // 2
+    swap = half_ref[0] != 0
+    for n in range(2):
+        mine = slice(n * (rows // 2), (n + 1) * (rows // 2))
+        terms = refs[3 * n : 3 * n + 3]
+        total = terms[0][...].astype(jnp.float32) + terms[1][...].astype(jnp.float32)
+        total = (total + terms[2][...].astype(jnp.float32)).astype(jnp.bfloat16)
+        for i in range(tiles):
+            near = total[:, i * part : (i + 1) * part]
+            far = total[:, width // 2 + i * part : width // 2 + (i + 1) * part]
+            out_ref[mine, (2 * i) * part : (2 * i + 1) * part] = jnp.where(swap, far, near)
+            out_ref[mine, (2 * i + 1) * part : (2 * i + 2) * part] = jnp.where(swap, near, far)
+
+
+def finish(half, terms, tiles):
+    rows, width = terms[0].shape
+    return pl.pallas_call(
+        functools.partial(finish_kernel, tiles),
+        in_specs=[IN_SMEM] + [IN_VMEM] * len(terms),
+        out_specs=IN_VMEM,
+        out_shape=jax.ShapeDtypeStruct((2 * rows, width), jnp.bfloat16),
+        compiler_params=SMALL_GRANT,
+        name="finish",
+    )(half, *terms)
+
+
+def serve_kernel(fs_count, tp_count, gate_rows, down_at, half_ref, low_ref, high_ref, gate_ref, up_ref, down_ref):
+    part = low_ref.shape[1] // fs_count
+    swap = half_ref[0] != 0
+    for f in range(fs_count):
+        cols = slice(f * part, (f + 1) * part)
+        for n, ref in enumerate((gate_ref, up_ref)):
+            rows = slice(n * gate_rows, (n + 1) * gate_rows)
+            near, far = low_ref[rows, cols], high_ref[rows, cols]
+            ref[(2 * f) * part : (2 * f + 1) * part, :] = jnp.where(swap, far, near).T
+            ref[(2 * f + 1) * part : (2 * f + 2) * part, :] = jnp.where(swap, near, far).T
+    rows = slice(down_at, down_at + down_ref.shape[0])
+    part = low_ref.shape[1] // tp_count
+    for t in range(tp_count):
+        cols = slice(t * part, (t + 1) * part)
+        near, far = low_ref[rows, cols], high_ref[rows, cols]
+        down_ref[:, (2 * t) * part : (2 * t + 1) * part] = jnp.where(swap, far, near)
+        down_ref[:, (2 * t + 1) * part : (2 * t + 2) * part] = jnp.where(swap, near, far)
+
+
+def serve(half, low, high, fs_count, tp_count, gate_rows, down_at, down_rows):
+    width = 2 * low.shape[1]
+    tall = jax.ShapeDtypeStruct((width, gate_rows), jnp.bfloat16)
+    return pl.pallas_call(
+        functools.partial(serve_kernel, fs_count, tp_count, gate_rows, down_at),
+        in_specs=[IN_SMEM, IN_VMEM, IN_VMEM],
+        out_specs=[IN_VMEM] * 3,
+        out_shape=[tall, tall, jax.ShapeDtypeStruct((down_rows, width), jnp.bfloat16)],
+        compiler_params=SMALL_GRANT,
+        name="serve",
+    )(half, low, high)
+
+
+def held_kernel(order_ref, *refs):
+    tiles = refs[:-4]
+    gate_ref, up_ref, down_ref, stage_ref = refs[-4:]
+    units = tiles[0].shape[0] // 3
+    count = len(tiles)
+    width = tiles[0].shape[1]
+    for r in range(count):
+        spot = pl.multiple_of(order_ref[r] * units, units)
+        for m in range(3):
+            stage_ref[m, pl.ds(spot, units), :] = tiles[r][m * units : (m + 1) * units, :]
+    gate_ref[...] = stage_ref[0].T
+    up_ref[...] = stage_ref[1].T
+    for t in range(count):
+        down_ref[:, t * width : (t + 1) * width] = stage_ref[2, t * units : (t + 1) * units, :]
+
+
+def held_tiles(order, tiles):
+    count = len(tiles)
+    units, width = tiles[0].shape[0] // 3, tiles[0].shape[1]
+    tall = jax.ShapeDtypeStruct((width, count * units), jnp.bfloat16)
+    return pl.pallas_call(
+        held_kernel,
+        in_specs=[IN_SMEM] + [IN_VMEM] * count,
+        out_specs=[IN_VMEM] * 3,
+        out_shape=[tall, tall, jax.ShapeDtypeStruct((units, count * width), jnp.bfloat16)],
+        scratch_shapes=[pltpu.VMEM((3, count * units, width), jnp.bfloat16)],
+        compiler_params=SMALL_GRANT,
+        name="held_tiles",
+    )(order, *tiles)
+
+
+OUT_STREAMS = (("pa", 1, 0), ("nb", -1, 1), ("pb", 1, 1), ("na", -1, 0))
+
+
+def gather_plan(
+    tokens,
+    route_ids,
+    route_scores,
+    norm_gain,
+    expert_gate,
+    expert_up,
+    expert_down,
+    shared_gate,
+    shared_up,
+    shared_down,
+):
+    fs_count = lax.axis_size("fs")
+    tp_count = lax.axis_size("tp")
+    experts = fs_count * tp_count
+    ring = 2 * fs_count
+    hops = fs_count
+    half = lax.axis_index("grp").astype(jnp.int32)[None]
+    tp_index = lax.axis_index("tp").astype(jnp.int32)
+    me = lax.axis_index("fs").astype(jnp.int32) * tp_count + tp_index
+    own = jnp.stack([me, me ^ 1])
+
+    def spot(position, core):
+        position = position % ring
+        if position < fs_count:
+            return position * tp_count + core
+        return (ring - 1 - position) * tp_count + CORES + core
+
+    def around(value, way):
+        moves = [(spot(p, c), spot(p + way, c)) for p in range(ring) for c in range(CORES)]
+        return lax.ppermute(value, ("fs", "tp"), moves)
+
+    def across(value):
+        return lax.ppermute(value, "tp", [(i, i ^ 1) for i in range(tp_count)])
+
+    def sideways(value):
+        return lax.ppermute(value, "tp", [(i, i ^ CORES) for i in range(tp_count)])
+
+    gain = norm_gain[None, :]
+    gate_t = jnp.transpose(expert_gate, (0, 2, 1))
+    up_t = jnp.transpose(expert_up, (0, 2, 1))
+    sg_t, su_t = shared_gate.T, shared_up.T
+    units = gate_t.shape[1]
+    share = sg_t.shape[0] // experts
+    packed = pack_tiles(half, gate_t, up_t, expert_down, sg_t, su_t, shared_down, gain)
+    tail = packed.shape[1] - 3 * units
+    gate_rows, strip_rows = tp_count * units, tp_count * tail
+    down_rows = fs_count * units
+    down_at = 2 * gate_rows + strip_rows
+    landed = lax.all_to_all(packed, ("fs", "tp"), split_axis=0, concat_axis=0, tiled=True)
+    own_low = place_tiles(landed, fs_count, tp_count, units)
+    own_high = lax.ppermute(own_low, "grp", [(0, 1), (1, 0)])
+    peer_low = across(own_low)
+    peer_high = across(own_high)
+    mats = (own_low, peer_low, own_high, peer_high)
+
+    seen = {}
+    pair = norm_rows(half, tokens, route_ids, route_scores, experts, fs_count)
+    for name, _, n in OUT_STREAMS:
+        seen[name] = [pair[n]]
+    for s in range(1, hops + 1):
+        for name, way, _ in OUT_STREAMS:
+            if s < hops or name in ("pa", "nb"):
+                seen[name].append(around(seen[name][-1], way))
+
+    sizes = (gate_rows, strip_rows, down_rows, share, tail)
+    made = {name: {} for name in seen}
+    for s in range(hops, 0, -1):
+        keys = [(name, s) for name, _, _ in OUT_STREAMS if s < len(seen[name])]
+        if s == 1:
+            keys += [("pa", 0), ("pb", 0)]
+        outs = ffn(own, [seen[name][d] for name, d in keys], mats, experts, sizes)
+        for (name, d), out in zip(keys, outs):
+            made[name][d] = out
+
+    ended = {}
+    for name, way, _ in OUT_STREAMS:
+        deepest = max(made[name])
+        moving = made[name][deepest]
+        for d in range(deepest - 1, -1, -1):
+            moving = around(moving, -way)
+            if d > 0:
+                moving = (moving.astype(jnp.float32) + made[name][d].astype(jnp.float32)).astype(jnp.bfloat16)
+        ended[name] = moving
+    terms = (made["pa"][0], ended["pa"], ended["na"], made["pb"][0], ended["pb"], ended["nb"])
+    mixed = finish(half, terms, tp_count)
+
+    served_gate, served_up, served_down = serve(
+        half, own_low, own_high, fs_count, tp_count, gate_rows, down_at, down_rows
+    )
+
+    tile = jnp.concatenate([gain * sg_t, gain * su_t, shared_down], axis=0).astype(jnp.bfloat16)
+    tiles = [tile, sideways(tile)]
+    tiles += [across(tiles[0]), across(tiles[1])]
+    order = jnp.stack([tp_index, tp_index ^ CORES, tp_index ^ 1, tp_index ^ (CORES + 1)])
+    held_gate, held_up, held_down = held_tiles(order, tiles)
+    return (mixed, served_gate[None], served_up[None], served_down[None], held_gate, held_up, held_down)
+
+
+def gathers(experts, picks, groups, columns):
+    return experts <= 2 * picks and groups == 2 and columns == 2 * CORES
+
+
+def on_device(tokens, route_ids, *others):
+    fs_count, tp_count = lax.axis_size("fs"), lax.axis_size("tp")
+    if gathers(fs_count * tp_count, route_ids.shape[1], lax.axis_size("grp"), tp_count):
+        return gather_plan(tokens, route_ids, *others)
+    return exchange_plan(tokens, route_ids, *others)
 
 
 def solution(mesh):

time: 486 us -> 214 us (0.44)
  waiting for transfers between devices: 287 us -> 91.9 us
  blocking collectives: 79.3 us -> 45.2 us
  local copies, waits for them, and re-layouts: 42.8 us -> 12.6 us
  Pallas kernels: 0 us -> 29.5 us
  matrix products: 24.1 us -> 0 us
  other arithmetic: 19.1 us -> 2.98 us
  between operations: 13.9 us -> 0.89 us
  starting transfers between devices: 19.7 us -> 29.5 us
    all_to_all x4 -> x0, waiting for transfers between devices: 234 us -> none  [the longest x1 130 us: on_device(): lax.all_to_all(outbox.reshape(experts, capacity, width), ('fs', 'tp'), sp...]
    ppermute x0 -> x34, waiting for transfers between devices: none -> 91.9 us  [the longest x28 51.2 us: around(): return lax.ppermute(value, ('fs', 'tp'), moves)]
    all_gather x3 -> x0, waiting for transfers between devices: 52.7 us -> none  [the longest x1 52.7 us: on_device(): lax.all_gather(held_gate, 'fs', axis=0, tiled=True)]
    all_gather x3 -> x0, blocking collectives: 48.2 us -> none  [the longest x1 29.8 us: on_device(): lax.all_gather(tile_gate, 'tp', axis=1, tiled=True)]
    pallas_call x0 -> x10, Pallas kernels: none -> 29.5 us  [the longest x4 21.6 us: ffn(): pl.pallas_call(functools.partial(ffn_kernel, experts, *sizes, len(blocks)...]
    ppermute x0 -> x34, starting transfers between devices: none -> 29.5 us  [the longest x28 19.9 us: around(): return lax.ppermute(value, ('fs', 'tp'), moves)]
    dot_general x4 -> x0, matrix products: 24.1 us -> none  [the longest x1 12.9 us: expert_rows(): jnp.dot(hidden, w_down, preferred_element_type=jnp.float32)]
    all_to_all x4 -> x0, starting transfers between devices: 19.6 us -> none  [the longest x1 5.04 us: on_device(): lax.all_to_all(piece_up[:, None], ('fs', 'tp'), split_axis=0, concat_axis...]
  transfers between devices with their start and end apart: 7 -> 34, of which waited for: 5 -> 16; matrix products, arithmetic and copies ran while one was open for 12% -> 1% of each run, Pallas kernels for 0% -> 13%
where the time goes in v2:
time: 214 us; the launch traced here: 213 us
  waiting for transfers between devices  91.9 us (43%)
  blocking collectives  45.2 us (21%)
  Pallas kernels  29.5 us (14%)
  starting transfers between devices  29.5 us (14%)
  local copies, waits for them, and re-layouts  12.6 us (6%)
  other arithmetic  2.98 us (1%)
    ppermute x28, waiting for transfers between devices, around(): return lax.ppermute(value, ('fs', 'tp'), moves)  51.2 us
    all_to_all x1, blocking collectives, gather_plan(): lax.all_to_all(packed, ('fs', 'tp'), split_axis=0, concat_axis=0, tiled=T...  45.2 us
    ppermute x1, waiting for transfers between devices, gather_plan(): own_high = lax.ppermute(own_low, 'grp', [(0, 1), (1, 0)])  39.5 us
    pallas_call x4, Pallas kernels, ffn(): pl.pallas_call(functools.partial(ffn_kernel, experts, *sizes, len(blocks)...  21.6 us
    ppermute x28, starting transfers between devices, around(): return lax.ppermute(value, ('fs', 'tp'), moves)  19.9 us
    unnamed x50, local copies, waits for them, and re-layouts  12.6 us
    ppermute x4, starting transfers between devices, across(): return lax.ppermute(value, 'tp', [(i, i ^ 1) for i in range(tp_count)])  7.1 us
  transfers between devices with their start and end apart: 34, of which 16 were waited for; matrix products, arithmetic and copies ran while one was open for 1% of the time, Pallas kernels for 13%

profile of v2, /device:TPU:11, one launch (start us, length us, event | category | flops | bytes accessed | tf_op | source)
XLA Modules:
  0.0 212.5 jit_solution(451011853493635900)
XLA Ops:
  0.6 1.6 copy-done
  2.2 1.6 copy-done.1
  3.8 1.6 copy-done.2
  9.5 45.2 %all_to_all.5.in_ref = bf16[16,208,256]{2,1,0:T(8,128)(2,1)S(1)} all-to-all(bf16[16,208,256]{2,1,0:T(8,128)(2,1)S(1)} %pack_tiles.1), channel_id=1, replica_groups=mesh['grp'=2,'fs'=4,'tp'=4] {'fs','tp'}, dimensions={0} | all-to-all | bytes 3407872 | tf_op jit(solution)/shard_map/all_to_all | solution.py:453
  56.8 39.5 %collective-permute-done.5.refs_8_.refs_4_.refs_6_.high_ref = bf16[896,1024]{1,0:T(8,128)(2,1)} collective-permute-done((bf16[896,1024]{1,0:T(8,128)(2,1)S(1)}, bf16[896,1024]{1,0:T(8,128)(2,1)}, u32[]{:S(2)}, u32[]{:S(2)}) %collective-permute-start.5) | collective-permute-done | bytes 1835040 | tf_op jit(solution)/shard_map/ppermute | solution.py:455
  100.3 5.7 %collective-permute-done.refs_0_ = bf16[64,2176]{1,0:T(8,128)(2,1)S(1)} collective-permute-done((bf16[64,2176]{1,0:T(8,128)(2,1)S(1)}, bf16[64,2176]{1,0:T(8,128)(2,1)S(1)}, u32[]{:S(2)}, u32[]{:S(2)}) %collective-permute-start) | collective-permute-done | bytes 278560 | tf_op jit(solution)/shard_map/ppermute | solution.py:434
  107.8 4.3 %collective-permute-done.2.refs_2_ = bf16[64,2176]{1,0:T(8,128)(2,1)S(1)} collective-permute-done((bf16[64,2176]{1,0:T(8,128)(2,1)S(1)}, bf16[64,2176]{1,0:T(8,128)(2,1)S(1)}, u32[]{:S(2)}, u32[]{:S(2)}) %collective-permute-start.2) | collective-permute-done | bytes 278560 | tf_op jit(solution)/shard_map/ppermute | solution.py:434
  114.0 4.0 %collective-permute-done.7.refs_0_ = bf16[64,2176]{1,0:T(8,128)(2,1)S(1)} collective-permute-done((bf16[64,2176]{1,0:T(8,128)(2,1)S(1)}, bf16[64,2176]{1,0:T(8,128)(2,1)S(1)}, u32[]{:S(2)}, u32[]{:S(2)}) %collective-permute-start.7) | collective-permute-done | bytes 278560 | tf_op jit(solution)/shard_map/ppermute | solution.py:434
  120.8 3.1 %collective-permute-done.14.refs_2_ = bf16[64,2176]{1,0:T(8,128)(2,1)S(1)} collective-permute-done((bf16[64,2176]{1,0:T(8,128)(2,1)S(1)}, bf16[64,2176]{1,0:T(8,128)(2,1)S(1)}, u32[]{:S(2)}, u32[]{:S(2)}) %collective-permute-start.14) | collective-permute-done | bytes 278560 | tf_op jit(solution)/shard_map/ppermute | solution.py:434
  124.2 5.8 %collective-permute-done.8.refs_0_ = bf16[64,2176]{1,0:T(8,128)(2,1)} collective-permute-done((bf16[64,2176]{1,0:T(8,128)(2,1)S(1)}, bf16[64,2176]{1,0:T(8,128)(2,1)}, u32[]{:S(2)}, u32[]{:S(2)}) %collective-permute-start.8) | collective-permute-done | bytes 278560 | tf_op jit(solution)/shard_map/ppermute | solution.py:434
  131.6 1.3 collective-permute-done.16.refs_3_
  133.9 3.7 %collective-permute-done.9.refs_0_ = bf16[64,2176]{1,0:T(8,128)(2,1)} collective-permute-done((bf16[64,2176]{1,0:T(8,128)(2,1)}, bf16[64,2176]{1,0:T(8,128)(2,1)}, u32[]{:S(2)}, u32[]{:S(2)}) %collective-permute-start.9) | collective-permute-done | bytes 278560 | tf_op jit(solution)/shard_map/ppermute | solution.py:434
  139.2 4.9 %expert_ffn.5 = (bf16[64,2048]{1,0:T(8,128)(2,1)S(1)}, bf16[64,2048]{1,0:T(8,128)(2,1)S(1)}) custom-call(s32[2]{0:T(128)S(1)} %pad_add_fusion.own_ref, bf16[64,2176]{1,0:T(8,128)(2,1)} %collective-permute-done.9.refs_0_, bf16[64,2176]{1,0:T(8,128)(2,1)} %collective-permute-done.12.refs_1_, bf16[896,1024]{1,0:T(8,128)(2,1)S(1)} %place_tiles.1.refs_6_.refs_2_.refs_4_.low_ref, ...), custom_call_target="tpu_custom_call" | custom-call | tf_op jit(solution)/shard_map/expert_ffn/pallas_call | solution.py:299
  145.9 3.3 %collective-permute-start.32 = (bf16[192,512]{1,0:T(8,128)(2,1)S(1)}, bf16[192,512]{1,0:T(8,128)(2,1)S(1)}, u32[]{:S(2)}, u32[]{:S(2)}) collective-permute-start(bf16[192,512]{1,0:T(8,128)(2,1)S(1)} %pad_maximum_fusion.refs_0_), channel_id=1, source_target_pairs={{0,1},{1,0},{2,3},{3,2},{4,5},{5,4},{6,7},{7,6},{8,9},{9,8},{10,11... | collective-permute-start | bytes 589832 | tf_op jit(solution)/shard_map/ppermute | solution.py:437
  149.2 5.3 %expert_ffn.6 = (bf16[64,2048]{1,0:T(8,128)(2,1)S(1)}, bf16[64,2048]{1,0:T(8,128)(2,1)S(1)}, bf16[64,2048]{1,0:T(8,128)(2,1)S(1)}, bf16[64,2048]{1,0:T(8,128)(2,1)S(1)}) custom-call(s32[2]{0:T(128)S(1)} %pad_add_fusion.own_ref, bf16[64,2176]{1,0:T(8,128)(2,1)} %collective-permute-done.8.refs_0_, bf16[64,2176]{1,0:T(8,128)(2,1)} %collective-permute-done.11.refs_1_, ...), custom_call_target="tpu_custom_call" | custom-call | tf_op jit(solution)/shard_map/expert_ffn/pallas_call | solution.py:299
  156.0 6.2 %expert_ffn.4 = (bf16[64,2048]{1,0:T(8,128)(2,1)S(1)}, bf16[64,2048]{1,0:T(8,128)(2,1)S(1)}, bf16[64,2048]{1,0:T(8,128)(2,1)S(1)}, bf16[64,2048]{1,0:T(8,128)(2,...) custom-call(s32[2]{0:T(128)S(1)} %pad_add_fusion.own_ref, ...), custom_call_target="tpu_custom_call" | custom-call | tf_op jit(solution)/shard_map/expert_ffn/pallas_call | solution.py:299
  163.6 5.2 %expert_ffn.7 = (bf16[64,2048]{1,0:T(8,128)(2,1)S(1)}, bf16[64,2048]{1,0:T(8,128)(2,1)S(1)}, bf16[64,2048]{1,0:T(8,128)(2,1)S(1)}, bf16[64,2048]{1,0:T(8,128)(2,1)S(1)}) custom-call(s32[2]{0:T(128)S(1)} %pad_add_fusion.own_ref, bf16[64,2176]{1,0:T(8,128)(2,1)S(1)} %copy-done.10, bf16[64,2176]{1,0:T(8,128)(2,1)S(1)} %copy-done.12, ...), custom_call_target="tpu_custom_call" | custom-call | tf_op jit(solution)/shard_map/expert_ffn/pallas_call | solution.py:299
  171.3 4.9 %collective-permute-done.27 = bf16[64,2048]{1,0:T(8,128)(2,1)S(1)} collective-permute-done((bf16[64,2048]{1,0:T(8,128)(2,1)S(1)}, bf16[64,2048]{1,0:T(8,128)(2,1)S(1)}, u32[]{:S(2)}, u32[]{:S(2)}) %collective-permute-start.27) | collective-permute-done | bytes 262176 | tf_op jit(solution)/shard_map/ppermute | solution.py:434
  177.8 4.0 %collective-permute-done.22 = bf16[64,2048]{1,0:T(8,128)(2,1)S(1)} collective-permute-done((bf16[64,2048]{1,0:T(8,128)(2,1)S(1)}, bf16[64,2048]{1,0:T(8,128)(2,1)S(1)}, u32[]{:S(2)}, u32[]{:S(2)}) %collective-permute-start.22) | collective-permute-done | bytes 262176 | tf_op jit(solution)/shard_map/ppermute | solution.py:434
  184.2 3.2 %collective-permute-done.28 = bf16[64,2048]{1,0:T(8,128)(2,1)S(1)} collective-permute-done((bf16[64,2048]{1,0:T(8,128)(2,1)S(1)}, bf16[64,2048]{1,0:T(8,128)(2,1)S(1)}, u32[]{:S(2)}, u32[]{:S(2)}) %collective-permute-start.28) | collective-permute-done | bytes 262176 | tf_op jit(solution)/shard_map/ppermute | solution.py:434
  189.7 8.9 %collective-permute-done.29 = bf16[64,2048]{1,0:T(8,128)(2,1)S(1)} collective-permute-done((bf16[64,2048]{1,0:T(8,128)(2,1)S(1)}, bf16[64,2048]{1,0:T(8,128)(2,1)S(1)}, u32[]{:S(2)}, u32[]{:S(2)}) %collective-permute-start.29) | collective-permute-done | bytes 262176 | tf_op jit(solution)/shard_map/ppermute | solution.py:434
  201.5 2.0 collective-permute-start.33
  205.7 2.0 held_tiles.1
  207.7 3.8 %serve.1 = (bf16[2048,256]{1,0:T(8,128)(2,1)}, bf16[2048,256]{1,0:T(8,128)(2,1)}, bf16[256,2048]{1,0:T(8,128)(2,1)}) custom-call(s32[1]{0:T(128)} %bitcast.half_ref, bf16[896,1024]{1,0:T(8,128)(2,1)S(1)} %place_tiles.1.refs_6_.refs_2_.refs_4_.low_ref, bf16[896,1024]{1,0:T(8,128)(2,1)} %collective-permute-done.5.refs_8_.refs_4_.refs_6_.high_ref), custom_call_target="tpu_custom_call" | custom-call | tf_op jit(solution)/shard_map/serve/pallas_call | solution.py:360
  (120 shorter events, 40.8 us)
Async XLA Ops:
  54.9 41.4 %collective-permute-start.5 = (bf16[896,1024]{1,0:T(8,128)(2,1)S(1)}, bf16[896,1024]{1,0:T(8,128)(2,1)}, u32[]{:S(2)}, u32[]{:S(2)}) collective-permute-start(bf16[896,1024]{1,0:T(8,128)(2,1)S(1)} %place_tiles.1.refs_6_.refs_2_.refs_4_.low_ref), channel_id=1, source_target_pairs={{0,16},{16,0},{1,17},{17,1},{2,18},{18,2},{3,19},{19,3},{4,20},{20... | collective-permute-start | bytes 5505032 | tf_op jit(solution)/shard_map/ppermute | solution.py:455
  56.2 82.9 %collective-permute-start.4 = (bf16[896,1024]{1,0:T(8,128)(2,1)S(1)}, bf16[896,1024]{1,0:T(8,128)(2,1)}, u32[]{:S(2)}, u32[]{:S(2)}) collective-permute-start(bf16[896,1024]{1,0:T(8,128)(2,1)S(1)} %place_tiles.1.refs_6_.refs_2_.refs_4_.low_ref), channel_id=1, source_target_pairs={{0,1},{1,0},{2,3},{3,2},{4,5},{5,4},{6,7},{7,6},{8,9},{9,8},{10,11... | collective-permute-start | bytes 5505032 | tf_op jit(solution)/shard_map/ppermute | solution.py:437
  96.3 42.9 %collective-permute-start.6 = (bf16[896,1024]{1,0:T(8,128)(2,1)}, bf16[896,1024]{1,0:T(8,128)(2,1)}, u32[]{:S(2)}, u32[]{:S(2)}) collective-permute-start(bf16[896,1024]{1,0:T(8,128)(2,1)} %collective-permute-done.5.refs_8_.refs_4_.refs_6_.high_ref), channel_id=1, source_target_pairs={{0,1},{1,0},{2,3},{3,2},{4,5},{5,4},{6,7},{7,6},{8,9},{9,8},{10,11... | collective-permute-start | bytes 5505032 | tf_op jit(solution)/shard_map/ppermute | solution.py:437
  97.8 8.3 %collective-permute-start = (bf16[64,2176]{1,0:T(8,128)(2,1)S(1)}, bf16[64,2176]{1,0:T(8,128)(2,1)S(1)}, u32[]{:S(2)}, u32[]{:S(2)}) collective-permute-start(bf16[64,2176]{1,0:T(8,128)(2,1)S(1)} %get-tuple-element.31.refs_4_), channel_id=1, source_target_pairs={{0,4},{1,5},{4,8},{5,9},{8,12},{9,13},{12,14},{13,15},{14,10},{15,... | collective-permute-start | bytes 835592 | tf_op jit(solution)/shard_map/ppermute | solution.py:434
  99.3 12.8 %collective-permute-start.2 = (bf16[64,2176]{1,0:T(8,128)(2,1)S(1)}, bf16[64,2176]{1,0:T(8,128)(2,1)S(1)}, u32[]{:S(2)}, u32[]{:S(2)}) collective-permute-start(bf16[64,2176]{1,0:T(8,128)(2,1)S(1)} %get-tuple-element.32.refs_5_), channel_id=1, source_target_pairs={{0,4},{1,5},{4,8},{5,9},{8,12},{9,13},{12,14},{13,15},{14,10},{15,... | collective-permute-start | bytes 835592 | tf_op jit(solution)/shard_map/ppermute | solution.py:434
  106.7 11.2 %collective-permute-start.7 = (bf16[64,2176]{1,0:T(8,128)(2,1)S(1)}, bf16[64,2176]{1,0:T(8,128)(2,1)S(1)}, u32[]{:S(2)}, u32[]{:S(2)}) collective-permute-start(bf16[64,2176]{1,0:T(8,128)(2,1)S(1)} %collective-permute-done.refs_0_), channel_id=1, source_target_pairs={{0,4},{1,5},{4,8},{5,9},{8,12},{9,13},{12,14},{13,15},{14,10},{15,... | collective-permute-start | bytes 835592 | tf_op jit(solution)/shard_map/ppermute | solution.py:434
  113.0 10.9 %collective-permute-start.14 = (bf16[64,2176]{1,0:T(8,128)(2,1)S(1)}, bf16[64,2176]{1,0:T(8,128)(2,1)S(1)}, u32[]{:S(2)}, u32[]{:S(2)}) collective-permute-start(bf16[64,2176]{1,0:T(8,128)(2,1)S(1)} %collective-permute-done.2.refs_2_), channel_id=1, source_target_pairs={{0,4},{1,5},{4,8},{5,9},{8,12},{9,13},{12,14},{13,15},{14,10},{15,... | collective-permute-start | bytes 835592 | tf_op jit(solution)/shard_map/ppermute | solution.py:434
  118.0 12.0 %collective-permute-start.8 = (bf16[64,2176]{1,0:T(8,128)(2,1)S(1)}, bf16[64,2176]{1,0:T(8,128)(2,1)}, u32[]{:S(2)}, u32[]{:S(2)}) collective-permute-start(bf16[64,2176]{1,0:T(8,128)(2,1)S(1)} %collective-permute-done.7.refs_0_), channel_id=1, source_target_pairs={{0,4},{1,5},{4,8},{5,9},{8,12},{9,13},{12,14},{13,15},{14,10},{15,... | collective-permute-start | bytes 835592 | tf_op jit(solution)/shard_map/ppermute | solution.py:434
  119.7 11.3 %collective-permute-start.11 = (bf16[64,2176]{1,0:T(8,128)(2,1)S(1)}, bf16[64,2176]{1,0:T(8,128)(2,1)}, u32[]{:S(2)}, u32[]{:S(2)}) collective-permute-start(bf16[64,2176]{1,0:T(8,128)(2,1)S(1)} %collective-permute-done.10.refs_1_), channel_id=1, source_target_pairs={{0,2},{1,3},{4,0},{5,1},{8,4},{9,5},{12,8},{13,9},{14,12},{15,13},... | collective-permute-start | bytes 835592 | tf_op jit(solution)/shard_map/ppermute | solution.py:434
  123.9 9.0 %collective-permute-start.16 = (bf16[64,2176]{1,0:T(8,128)(2,1)}, bf16[64,2176]{1,0:T(8,128)(2,1)}, u32[]{:S(2)}, u32[]{:S(2)}) collective-permute-start(bf16[64,2176]{1,0:T(8,128)(2,1)} %collective-permute-done.3.refs_3_), channel_id=1, source_target_pairs={{0,2},{1,3},{4,0},{5,1},{8,4},{9,5},{12,8},{13,9},{14,12},{15,13},... | collective-permute-start | bytes 835592 | tf_op jit(solution)/shard_map/ppermute | solution.py:434
  132.9 16.2 %collective-permute-start.15 = (bf16[64,2176]{1,0:T(8,128)(2,1)}, bf16[64,2176]{1,0:T(8,128)(2,1)S(1)}, u32[]{:S(2)}, u32[]{:S(2)}) collective-permute-start(bf16[64,2176]{1,0:T(8,128)(2,1)} %copy-done.13), channel_id=1, source_target_pairs={{0,4},{1,5},{4,8},{5,9},{8,12},{9,13},{12,14},{13,15},{14,10},{15,... | collective-permute-start | bytes 835592 | tf_op jit(solution)/shard_map/ppermute | solution.py:434
  137.7 11.5 %collective-permute-start.17 = (bf16[64,2176]{1,0:T(8,128)(2,1)}, bf16[64,2176]{1,0:T(8,128)(2,1)S(1)}, u32[]{:S(2)}, u32[]{:S(2)}) collective-permute-start(bf16[64,2176]{1,0:T(8,128)(2,1)} %collective-permute-done.16.refs_3_), channel_id=1, source_target_pairs={{0,2},{1,3},{4,0},{5,1},{8,4},{9,5},{12,8},{13,9},{14,12},{15,13},... | collective-permute-start | bytes 835592 | tf_op jit(solution)/shard_map/ppermute | solution.py:434
  144.1 24.7 %collective-permute-start.13 = (bf16[64,2048]{1,0:T(8,128)(2,1)S(1)}, bf16[64,2048]{1,0:T(8,128)(2,1)S(1)}, u32[]{:S(2)}, u32[]{:S(2)}) collective-permute-start(bf16[64,2048]{1,0:T(8,128)(2,1)S(1)} %get-tuple-element.34), channel_id=1, source_target_pairs={{0,2},{1,3},{4,0},{5,1},{8,4},{9,5},{12,8},{13,9},{14,12},{15,13},... | collective-permute-start | bytes 786440 | tf_op jit(solution)/shard_map/ppermute | solution.py:434
  144.7 55.8 %collective-permute-start.31 = (bf16[192,512]{1,0:T(8,128)(2,1)S(1)}, bf16[192,512]{1,0:T(8,128)(2,1)}, u32[]{:S(2)}, u32[]{:S(2)}) collective-permute-start(bf16[192,512]{1,0:T(8,128)(2,1)S(1)} %pad_maximum_fusion.refs_0_), channel_id=1, source_target_pairs={{0,2},{1,3},{2,0},{3,1},{4,6},{5,7},{6,4},{7,5},{8,10},{9,11},{10,... | collective-permute-start | bytes 589832 | tf_op jit(solution)/shard_map/ppermute | solution.py:440
  145.9 55.0 %collective-permute-start.32 = (bf16[192,512]{1,0:T(8,128)(2,1)S(1)}, bf16[192,512]{1,0:T(8,128)(2,1)S(1)}, u32[]{:S(2)}, u32[]{:S(2)}) collective-permute-start(bf16[192,512]{1,0:T(8,128)(2,1)S(1)} %pad_maximum_fusion.refs_0_), channel_id=1, source_target_pairs={{0,1},{1,0},{2,3},{3,2},{4,5},{5,4},{6,7},{7,6},{8,9},{9,8},{10,11... | collective-permute-start | bytes 589832 | tf_op jit(solution)/shard_map/ppermute | solution.py:437
  154.4 14.9 %collective-permute-start.21 = (bf16[64,2048]{1,0:T(8,128)(2,1)S(1)}, bf16[64,2048]{1,0:T(8,128)(2,1)S(1)}, u32[]{:S(2)}, u32[]{:S(2)}) collective-permute-start(bf16[64,2048]{1,0:T(8,128)(2,1)S(1)} %get-tuple-element.38), channel_id=1, source_target_pairs={{0,4},{1,5},{4,8},{5,9},{8,12},{9,13},{12,14},{13,15},{14,10},{15,... | collective-permute-start | bytes 786440 | tf_op jit(solution)/shard_map/ppermute | solution.py:434
  155.0 15.7 %collective-permute-start.24 = (bf16[64,2048]{1,0:T(8,128)(2,1)S(1)}, bf16[64,2048]{1,0:T(8,128)(2,1)S(1)}, u32[]{:S(2)}, u32[]{:S(2)}) collective-permute-start(bf16[64,2048]{1,0:T(8,128)(2,1)S(1)} %get-tuple-element.42), channel_id=1, source_target_pairs={{0,2},{1,3},{4,0},{5,1},{8,4},{9,5},{12,8},{13,9},{14,12},{15,13},... | collective-permute-start | bytes 786440 | tf_op jit(solution)/shard_map/ppermute | solution.py:434
  170.7 11.1 %collective-permute-start.22 = (bf16[64,2048]{1,0:T(8,128)(2,1)S(1)}, bf16[64,2048]{1,0:T(8,128)(2,1)S(1)}, u32[]{:S(2)}, u32[]{:S(2)}) collective-permute-start(bf16[64,2048]{1,0:T(8,128)(2,1)S(1)} %add_convert_fusion.6), channel_id=1, source_target_pairs={{0,4},{1,5},{4,8},{5,9},{8,12},{9,13},{12,14},{13,15},{14,10},{15,... | collective-permute-start | bytes 786440 | tf_op jit(solution)/shard_map/ppermute | solution.py:434
  177.3 10.1 %collective-permute-start.28 = (bf16[64,2048]{1,0:T(8,128)(2,1)S(1)}, bf16[64,2048]{1,0:T(8,128)(2,1)S(1)}, u32[]{:S(2)}, u32[]{:S(2)}) collective-permute-start(bf16[64,2048]{1,0:T(8,128)(2,1)S(1)} %add_convert_fusion.2), channel_id=1, source_target_pairs={{0,4},{1,5},{4,8},{5,9},{8,12},{9,13},{12,14},{13,15},{14,10},{15,... | collective-permute-start | bytes 786440 | tf_op jit(solution)/shard_map/ppermute | solution.py:434
  182.9 28.5 %collective-permute-start.23 = (bf16[64,2048]{1,0:T(8,128)(2,1)S(1)}, bf16[64,2048]{1,0:T(8,128)(2,1)S(1)}, u32[]{:S(2)}, u32[]{:S(2)}) collective-permute-start(bf16[64,2048]{1,0:T(8,128)(2,1)S(1)} %add_convert_fusion.5), channel_id=1, source_target_pairs={{0,4},{1,5},{4,8},{5,9},{8,12},{9,13},{12,14},{13,15},{14,10},{15,... | collective-permute-start | bytes 786440 | tf_op jit(solution)/shard_map/ppermute | solution.py:434
  187.4 24.1 %collective-permute-start.26 = (bf16[64,2048]{1,0:T(8,128)(2,1)}, bf16[64,2048]{1,0:T(8,128)(2,1)S(1)}, u32[]{:S(2)}, u32[]{:S(2)}) collective-permute-start(bf16[64,2048]{1,0:T(8,128)(2,1)} %add_convert_fusion.3), channel_id=1, source_target_pairs={{0,2},{1,3},{4,0},{5,1},{8,4},{9,5},{12,8},{13,9},{14,12},{15,13},... | collective-permute-start | bytes 786440 | tf_op jit(solution)/shard_map/ppermute | solution.py:434
  188.5 10.1 %collective-permute-start.29 = (bf16[64,2048]{1,0:T(8,128)(2,1)S(1)}, bf16[64,2048]{1,0:T(8,128)(2,1)S(1)}, u32[]{:S(2)}, u32[]{:S(2)}) collective-permute-start(bf16[64,2048]{1,0:T(8,128)(2,1)S(1)} %add_convert_fusion.1), channel_id=1, source_target_pairs={{0,4},{1,5},{4,8},{5,9},{8,12},{9,13},{12,14},{13,15},{14,10},{15,... | collective-permute-start | bytes 786440 | tf_op jit(solution)/shard_map/ppermute | solution.py:434
  198.6 12.9 %collective-permute-start.20 = (bf16[64,2048]{1,0:T(8,128)(2,1)}, bf16[64,2048]{1,0:T(8,128)(2,1)S(1)}, u32[]{:S(2)}, u32[]{:S(2)}) collective-permute-start(bf16[64,2048]{1,0:T(8,128)(2,1)} %add_convert_fusion.7), channel_id=1, source_target_pairs={{0,2},{1,3},{4,0},{5,1},{8,4},{9,5},{12,8},{13,9},{14,12},{15,13},... | collective-permute-start | bytes 786440 | tf_op jit(solution)/shard_map/ppermute | solution.py:434
  200.5 11.0 %collective-permute-start.30 = (bf16[64,2048]{1,0:T(8,128)(2,1)}, bf16[64,2048]{1,0:T(8,128)(2,1)S(1)}, u32[]{:S(2)}, u32[]{:S(2)}) collective-permute-start(bf16[64,2048]{1,0:T(8,128)(2,1)} %add_convert_fusion), channel_id=1, source_target_pairs={{0,4},{1,5},{4,8},{5,9},{8,12},{9,13},{12,14},{13,15},{14,10},{15,... | collective-permute-start | bytes 786440 | tf_op jit(solution)/shard_map/ppermute | solution.py:434
  (35 other events, 291.3 us)
